TPU v7x, 128 devices: a whole 4x4x4 slice. The times are simulated.
128 devices in a mesh: sp: 32 (over z, y, core), tp: 4 (over x).
Axes of the slice: x: 4, y: 4, z: 4, core: 2. Of those that a mesh axis runs over, the one named last changes fastest.
Arguments:
- resid: bfloat16 [16384, 2048], P(('sp', 'tp')), may hold values from -6 to 6
- query: bfloat16 [16384, 2048], P('sp', 'tp'), may hold values from -6 to 6
- forget_logits: bfloat16 [16384, 2048], P('sp', 'tp'), may hold values from -5 to 5
- forget_margin: float32 [2048], P('tp'), may hold values from 0 to 0.07, as said below
- decay_spike: float32 [16384, 16], P('sp', 'tp'), may hold values from -0.75 to 0
- value_logits: bfloat16 [16384, 2048], P('sp', 'tp'), may hold values from -6 to 6
- output_gate_logits: bfloat16 [16384, 2048], P('sp', 'tp'), may hold values from -6 to 6
- head_norm_scale: float32 [2048], P('tp'), may hold values from 0.1 to 1.9
- output_matrix: bfloat16 [2048, 2048], replicated, may hold values from -0.125 to 0.125
- norm_scale_vector: float32 [2048], replicated, may hold values from 0.1 to 1.9
- routes: int32 [16384, 2], P(('sp', 'tp')), may hold values from 0 to 127, all different within a row; in each aligned block of 128 rows (0 to 127, 128 to 255, ...) at most 4 rows name the same one
- routing_weight: float32 [16384, 2], P(('sp', 'tp')), may hold values from 0.2 to 1
- gate_matrix: bfloat16 [128, 2048, 1024], P(('sp', 'tp')), may hold values from -0.125 to 0.125
- up_matrix: bfloat16 [128, 2048, 1024], P(('sp', 'tp')), may hold values from -0.125 to 0.125
- down_matrix: bfloat16 [128, 1024, 2048], P(('sp', 'tp')), may hold values from -0.1875 to 0.1875
Outputs:
- result: bfloat16 [16384, 2048], P(('sp', 'tp'))
Inputs may be any that keep to these rules, and one draw needn't show every extreme that they name: `routes`: within the rows of one device no expert is named by more than 4 rows; some device names some expert exactly 4 times in every draw. `forget_margin`: Positive.
All inputs are finite; a program needn't handle non-finite values.
Results may differ from a plain program's by a relative error of at most 0.012.
Values may be sent and summed in bfloat16 or wider, within the bound.
A program may use at most 128 MiB of HBM per device.

v0:
```python
import jax
import jax.numpy as jnp
from jax import lax
from jax.sharding import Mesh
from jax.sharding import PartitionSpec as P

DK = 128
BLOCK = 64
SP = ("sp_0", "sp_1", "sp_2")
SP_TP = ("sp_0", "sp_1", "sp_2", "tp")


maximum_value = lax.Precision.HIGHEST


def filled_with(value, identity):
    return jax.tree.map(
        lambda a, e: jnp.broadcast_to(jnp.asarray(e, a.dtype), a.shape), value, identity
    )


def carried_in(value, axes, combine, identity):
    before = start = filled_with(value, identity)
    so_far = value
    for axis in reversed(axes):
        devices, place = (lax.axis_size(axis), lax.axis_index(axis))
        pieces = jax.tree.map(lambda part: lax.all_gather(part, axis), so_far)
        inside, so_far = (start, start)
        for k in range(devices):
            passed = k < place
            so_far = combine(so_far, jax.tree.map(lambda part: part[k], pieces))
            inside = jax.tree.map(lambda new, old: jnp.where(passed, new, old), so_far, inside)
        before = combine(inside, before)
    return before


def in_blocks(value, dim, devices):
    lengths = value.shape
    parts = value.reshape(*lengths[:dim], devices, lengths[dim] // devices, *lengths[dim + 1 :])
    return jnp.moveaxis(parts, dim, 0)


def laid_out(parts, dim):
    parts = jnp.moveaxis(parts, 0, dim)
    lengths = parts.shape
    return parts.reshape(*lengths[:dim], lengths[dim] * lengths[dim + 1], *lengths[dim + 2 :])


def one_exchange(value, axis, axes, splits, concats):
    sizes = [lax.axis_size(a) for a in axes]
    parts = in_blocks(value, splits[0], sizes[0])
    parts = jnp.moveaxis(in_blocks(parts, splits[1] + 1, sizes[1]), 0, 1)
    inside = parts.shape[2:]
    parts = parts.reshape(-1, *inside)
    parts = lax.all_to_all(parts, axis, split_axis=0, concat_axis=0, tiled=True)
    parts = laid_out(parts.reshape(*sizes, *inside), concats[0] + 1)
    return laid_out(parts, concats[1])


def to_blocks(matrix, head_number):
    length, columns = matrix.shape
    return matrix.reshape(length // BLOCK, BLOCK, head_number, columns // head_number).transpose(
        0, 2, 1, 3
    )


def from_blocks(matrix):
    block_count, head_number, span_len, head_width = matrix.shape
    return matrix.transpose(0, 2, 1, 3).reshape(block_count * span_len, head_number * head_width)


def input_lookup(query, forget_logits, forget_margin, decay_spike, value_logits):
    head_number = decay_spike.shape[1]
    every_key = forget_margin[None, :] * jax.nn.sigmoid(-forget_logits.astype(jnp.float32))
    head_width = every_key.shape[1] // head_number
    logarithm_of_decay = jnp.log1p(-every_key) + jnp.repeat(decay_spike, head_width, axis=1)
    queries = query.astype(jnp.float32) * DK ** (-0.5)
    values = jax.nn.silu(value_logits.astype(jnp.float32))
    return (
        to_blocks(queries, head_number),
        to_blocks(every_key, head_number),
        to_blocks(values, head_number),
        to_blocks(logarithm_of_decay, head_number),
    )


def block_recurrence(queries, keys_in, values, logarithm_of_decay):
    span_len = queries.shape[2]
    causal = (
        lax.broadcasted_iota(jnp.int32, (span_len, span_len), 0)
        >= lax.broadcasted_iota(jnp.int32, (span_len, span_len), 1)
    )[:, :, None]
    cum_log = jnp.cumsum(logarithm_of_decay, axis=2)

    def advance(current_state, inputs):
        query_block, key_b, value_block, cumulative_block = inputs
        spread = cumulative_block[:, :, None, :] - cumulative_block[:, None, :, :]
        weight_t = jnp.where(causal, jnp.exp(jnp.where(causal, spread, 0.0)), 0.0)
        router_scores = jnp.einsum(
            "htk,hsk,htsk->hts", query_block, key_b, weight_t, precision=maximum_value
        )
        within = jnp.einsum("hts,hsv->htv", router_scores, value_block, precision=maximum_value)
        incoming_state = jnp.einsum(
            "bup,bpl->bul",
            query_block * jnp.exp(cumulative_block),
            current_state,
            precision=maximum_value,
        )
        final_block = cumulative_block[:, -1, :]
        decayed_state = key_b * jnp.exp(final_block[:, None, :] - cumulative_block)
        following_state = jnp.exp(final_block)[:, :, None] * current_state + jnp.einsum(
            "ixq,ixn->iqn", decayed_state, value_block, precision=maximum_value
        )
        return (following_state, within + incoming_state)

    start_state = jnp.zeros((queries.shape[1], queries.shape[3], values.shape[3]), jnp.float32)
    last_state, outputs = lax.scan(advance, start_state, (queries, keys_in, values, cum_log))
    return (last_state, outputs, cum_log)


def gate_rows(recurrence_output, output_gate_logits, head_norm_scale):
    square = jnp.mean(recurrence_output * recurrence_output, axis=3, keepdims=True)
    scaled = from_blocks(recurrence_output * lax.rsqrt(square + 1e-06)) * head_norm_scale[None, :]
    return (scaled * jax.nn.silu(output_gate_logits.astype(jnp.float32))).astype(jnp.bfloat16)


def row_norm(stream, norm_scale_vector):
    values = stream.astype(jnp.float32)
    square = jnp.mean(values * values, axis=1, keepdims=True)
    return (values * lax.rsqrt(square + 1e-06) * norm_scale_vector[None, :]).astype(jnp.bfloat16)


def join_states(earlier, later):
    early_log, early_state = earlier
    late_log, late_state = later
    return (early_log + late_log, jnp.exp(late_log)[:, :, None] * early_state + late_state)


def expert_block(slot_rows, gate_matrix, up_matrix, down_matrix):
    gate_part = jnp.einsum(
        "...ecd,edf->...ecf", slot_rows, gate_matrix, preferred_element_type=jnp.float32
    )
    up_part = jnp.einsum(
        "...ecd,edf->...ecf", slot_rows, up_matrix, preferred_element_type=jnp.float32
    )
    hidden = (jax.nn.silu(gate_part) * up_part).astype(jnp.bfloat16)
    return jnp.einsum(
        "...ecf,efd->...ecd", hidden, down_matrix, preferred_element_type=jnp.float32
    ).astype(jnp.bfloat16)


def body(
    resid,
    query,
    forget_logits,
    forget_margin,
    decay_spike,
    value_logits,
    output_gate_logits,
    head_norm_scale,
    output_matrix,
    norm_scale_vector,
    routes,
    routing_weight,
    gate_matrix,
    up_matrix,
    down_matrix,
):
    queries, keys_b, values, logarithm_of_decay = input_lookup(
        query, forget_logits, forget_margin, decay_spike, value_logits
    )
    last_state, recurrence_output, cum_log = block_recurrence(
        queries, keys_b, values, logarithm_of_decay
    )
    totals = cum_log[:, :, -1, :]
    before = jnp.cumsum(totals, axis=0) - totals
    device_log = jnp.sum(totals, axis=0)
    identity = (jnp.zeros_like(device_log), jnp.zeros_like(last_state))
    prior_state = carried_in((device_log, last_state), SP, join_states, identity)[1]
    readout_result = queries * jnp.exp(cum_log + before[:, :, None, :])
    recurrence_output = recurrence_output + jnp.einsum(
        "gwme,wej->gwmj", readout_result, prior_state, precision=maximum_value
    )
    gated_rows = gate_rows(recurrence_output, output_gate_logits, head_norm_scale)
    arrived_rows = lax.all_to_all(gated_rows, "tp", split_axis=0, concat_axis=1, tiled=True)
    mixed_rows = jnp.dot(arrived_rows, output_matrix, preferred_element_type=jnp.float32)
    stream = (resid.astype(jnp.float32) + mixed_rows).astype(jnp.bfloat16)
    normed = row_norm(stream, norm_scale_vector)
    row_count = routes.shape[0]
    top_count = routes.shape[1]
    model_width = normed.shape[1]
    per_device = gate_matrix.shape[0]
    devices = lax.axis_size(SP) * lax.axis_size("tp")
    experts = per_device * devices
    capacity = 2 * row_count * top_count // experts
    flat_routes = routes.reshape(-1)
    member = (flat_routes[:, None] == jnp.arange(experts, dtype=jnp.int32)[None, :]).astype(
        jnp.int32
    )
    slot_rank = jnp.sum(jnp.cumsum(member, axis=0) * member, axis=1) - 1
    position_entries = flat_routes * capacity + slot_rank
    select = (
        position_entries[:, None] == jnp.arange(experts * capacity, dtype=jnp.int32)[None, :]
    ).astype(jnp.bfloat16)
    select = select.reshape(row_count, top_count, experts * capacity)
    dispatch = jnp.sum(select, axis=1)
    packed = lax.dot_general(
        dispatch, normed, (((0,), (0,)), ((), ())), preferred_element_type=jnp.float32
    ).astype(jnp.bfloat16)
    sectioned = packed.reshape(
        lax.axis_size(SP), lax.axis_size("tp"), per_device, capacity, model_width
    )
    arrived = one_exchange(sectioned, SP_TP, (SP, "tp"), (0, 1), (0, 1))
    answers = expert_block(arrived, gate_matrix, up_matrix, down_matrix)
    returned = one_exchange(answers, SP_TP, (SP, "tp"), (0, 1), (0, 1))
    returned_rows = returned.reshape(experts * capacity, model_width)
    combined = stream.astype(jnp.float32)
    for pick_index in range(top_count):
        picked = jnp.dot(
            select[:, pick_index, :], returned_rows, preferred_element_type=jnp.float32
        )
        combined = combined + routing_weight[:, pick_index : pick_index + 1] * picked
    return combined.astype(jnp.bfloat16)


def solution(mesh):
    finer = Mesh(mesh.devices.reshape(4, 4, 2, mesh.shape["tp"]), ("sp_0", "sp_1", "sp_2", "tp"))
    placed = (
        P(SP_TP, None),
        P(SP, "tp"),
        P(SP, "tp"),
        P("tp"),
        P(SP, "tp"),
        P(SP, "tp"),
        P(SP, "tp"),
        P("tp"),
        P(),
        P(),
        P(SP_TP, None),
        P(SP_TP, None),
        P(SP_TP, None, None),
        P(SP_TP, None, None),
        P(SP_TP, None, None),
    )
    return jax.shard_map(
        body, mesh=finer, in_specs=placed, out_specs=P(SP_TP, None), check_vma=False
    )
```

profile of v0, /device:TPU:1, one launch (start us, length us, event | category | flops | bytes accessed | tf_op | source)
XLA Modules:
  0.0 324.6 jit_solution(18199731818932901205)
XLA Ops:
  8.0 2.6 divide_multiply_fusion
  14.9 1.4 reshape.287
  17.4 1.6 reshape.288
  20.2 113.1 %while.14 = (s32[]{:T(128)}, f32[4,128,128]{2,1,0:T(8,128)S(1)}, f32[8,4,64,128]{3,2,0,1:T(8,128)}, f32[8,4,64,128]{3,0,1,2:T(8,128)S(1)}, f32[8,4,64,128]{3,1,2...) while((s32[]{:T(128)}, f32[4,128,128]{2,1,0:T(8,128)S(1)}, ...), condition=%wide.region_2.3_spmd.clone.clone, body=%wide.region_1.2_spmd.clone.clone.sunk | while | flops 138792960 | bytes 20862588 | solution.py:117
  20.3 1.7 exponential_select_fusion.2
  23.9 7.3 %fusion.164 = f32[4,64,64]{1,2,0:T(8,128)S(1)} fusion(f32[4,64,64,128]{3,2,1,0:T(8,128)S(1)} %exponential_select_fusion.2, f32[4,128,64]{1,2,0:T(8,128)S(1)} %dynamic-slice_bitcast_fusion.2, f32[4,128,64]{1,2,0:T(8,128)S(1)} %bitcast.352), kind=kLoop, calls=%fused_computation.2.clone.1 | loop fusion | flops 6275072 | bytes 8716288 | tf_op jit(solution)/shard_map/while/body/eval_jaxpr/htk,hsk,htsk->hts/dot_general | solution.py:99
  31.7 1.9 fusion.166
  34.4 1.7 exponential_select_fusion.2
  38.1 7.3 %fusion.164 = f32[4,64,64]{1,2,0:T(8,128)S(1)} fusion(f32[4,64,64,128]{3,2,1,0:T(8,128)S(1)} %exponential_select_fusion.2, f32[4,128,64]{1,2,0:T(8,128)S(1)} %dynamic-slice_bitcast_fusion.2, f32[4,128,64]{1,2,0:T(8,128)S(1)} %bitcast.352), kind=kLoop, calls=%fused_computation.2.clone.1 | loop fusion | flops 6275072 | bytes 8716288 | tf_op jit(solution)/shard_map/while/body/eval_jaxpr/htk,hsk,htsk->hts/dot_general | solution.py:99
  45.8 1.9 fusion.166
  48.6 1.7 exponential_select_fusion.2
  52.2 7.3 %fusion.164 = f32[4,64,64]{1,2,0:T(8,128)S(1)} fusion(f32[4,64,64,128]{3,2,1,0:T(8,128)S(1)} %exponential_select_fusion.2, f32[4,128,64]{1,2,0:T(8,128)S(1)} %dynamic-slice_bitcast_fusion.2, f32[4,128,64]{1,2,0:T(8,128)S(1)} %bitcast.352), kind=kLoop, calls=%fused_computation.2.clone.1 | loop fusion | flops 6275072 | bytes 8716288 | tf_op jit(solution)/shard_map/while/body/eval_jaxpr/htk,hsk,htsk->hts/dot_general | solution.py:99
  59.9 1.9 fusion.166
  62.7 1.7 exponential_select_fusion.2
  66.4 7.3 %fusion.164 = f32[4,64,64]{1,2,0:T(8,128)S(1)} fusion(f32[4,64,64,128]{3,2,1,0:T(8,128)S(1)} %exponential_select_fusion.2, f32[4,128,64]{1,2,0:T(8,128)S(1)} %dynamic-slice_bitcast_fusion.2, f32[4,128,64]{1,2,0:T(8,128)S(1)} %bitcast.352), kind=kLoop, calls=%fused_computation.2.clone.1 | loop fusion | flops 6275072 | bytes 8716288 | tf_op jit(solution)/shard_map/while/body/eval_jaxpr/htk,hsk,htsk->hts/dot_general | solution.py:99
  74.1 1.9 fusion.166
  76.9 1.7 exponential_select_fusion.2
  80.5 7.3 %fusion.164 = f32[4,64,64]{1,2,0:T(8,128)S(1)} fusion(f32[4,64,64,128]{3,2,1,0:T(8,128)S(1)} %exponential_select_fusion.2, f32[4,128,64]{1,2,0:T(8,128)S(1)} %dynamic-slice_bitcast_fusion.2, f32[4,128,64]{1,2,0:T(8,128)S(1)} %bitcast.352), kind=kLoop, calls=%fused_computation.2.clone.1 | loop fusion | flops 6275072 | bytes 8716288 | tf_op jit(solution)/shard_map/while/body/eval_jaxpr/htk,hsk,htsk->hts/dot_general | solution.py:99
  88.2 1.9 fusion.166
  91.0 1.7 exponential_select_fusion.2
  94.6 7.3 %fusion.164 = f32[4,64,64]{1,2,0:T(8,128)S(1)} fusion(f32[4,64,64,128]{3,2,1,0:T(8,128)S(1)} %exponential_select_fusion.2, f32[4,128,64]{1,2,0:T(8,128)S(1)} %dynamic-slice_bitcast_fusion.2, f32[4,128,64]{1,2,0:T(8,128)S(1)} %bitcast.352), kind=kLoop, calls=%fused_computation.2.clone.1 | loop fusion | flops 6275072 | bytes 8716288 | tf_op jit(solution)/shard_map/while/body/eval_jaxpr/htk,hsk,htsk->hts/dot_general | solution.py:99
  102.4 1.9 fusion.166
  105.1 1.7 exponential_select_fusion.2
  108.8 7.3 %fusion.164 = f32[4,64,64]{1,2,0:T(8,128)S(1)} fusion(f32[4,64,64,128]{3,2,1,0:T(8,128)S(1)} %exponential_select_fusion.2, f32[4,128,64]{1,2,0:T(8,128)S(1)} %dynamic-slice_bitcast_fusion.2, f32[4,128,64]{1,2,0:T(8,128)S(1)} %bitcast.352), kind=kLoop, calls=%fused_computation.2.clone.1 | loop fusion | flops 6275072 | bytes 8716288 | tf_op jit(solution)/shard_map/while/body/eval_jaxpr/htk,hsk,htsk->hts/dot_general | solution.py:99
  116.5 1.9 fusion.166
  119.3 1.7 exponential_select_fusion.2
  122.9 7.3 %fusion.164 = f32[4,64,64]{1,2,0:T(8,128)S(1)} fusion(f32[4,64,64,128]{3,2,1,0:T(8,128)S(1)} %exponential_select_fusion.2, f32[4,128,64]{1,2,0:T(8,128)S(1)} %dynamic-slice_bitcast_fusion.2, f32[4,128,64]{1,2,0:T(8,128)S(1)} %bitcast.352), kind=kLoop, calls=%fused_computation.2.clone.1 | loop fusion | flops 6275072 | bytes 8716288 | tf_op jit(solution)/shard_map/while/body/eval_jaxpr/htk,hsk,htsk->hts/dot_general | solution.py:99
  130.6 1.9 fusion.166
  133.3 3.2 all-gather.1
  136.5 1.9 all-gather.3
  139.4 8.8 %all-gather.4 = f32[4,4,128]{2,1,0:T(4,128)S(1)} all-gather(f32[1,4,128]{2,1,0:T(4,128)S(1)} %get-tuple-element.149), channel_id=4, replica_groups=mesh['sp_0'=4,'sp_1'=4,'sp_2'=2,'tp'=4] {'sp_1'}, dimensions={0}, use_global_device_ids=true | all-gather | bytes 10240 | tf_op jit(solution)/shard_map/all_gather | solution.py:27
  148.2 15.5 %all-gather.8.cloned.1.call-done = f32[4,4,128,128]{3,2,1,0:T(8,128)} async-done(((f32[1,4,128,128]{3,2,1,0:T(8,128)}), f32[4,4,128,128]{3,2,1,0:T(8,128)}) %all-gather.8.cloned.1.call-update) | async-done | bytes 1048592 | tf_op jit(solution)/shard_map/all_gather | solution.py:27
  163.7 2.2 multiply_add_fusion
  166.8 8.8 %all_gather.31 = f32[4,4,128]{2,1,0:T(4,128)S(1)} all-gather(f32[1,4,128]{2,1,0:T(4,128)S(1)} %get-tuple-element.157), channel_id=1, replica_groups=mesh['sp_0'=4,'sp_1'=4,'sp_2'=2,'tp'=4] {'sp_0'}, dimensions={0}, use_global_device_ids=true | all-gather | bytes 10240 | tf_op jit(solution)/shard_map/all_gather | solution.py:27
  175.8 1.7 bitcast_multiply_fusion.8
  177.4 13.3 %all-gather.10.cloned.1.call-done = f32[4,4,128,128]{3,2,1,0:T(8,128)} async-done(((f32[1,4,128,128]{3,2,1,0:T(8,128)}), f32[4,4,128,128]{3,2,1,0:T(8,128)}) %all-gather.10.cloned.1.call-update) | async-done | bytes 1048592 | tf_op jit(solution)/shard_map/all_gather | solution.py:27
  190.7 4.7 %multiply_reduce_fusion.1 = (f32[8,4,64]{2,0,1:T(8,128)S(1)}, f32[8,4,64,128]{3,2,0,1:T(8,128)S(1)}) fusion(f32[8,4,64,128]{3,2,0,1:T(8,128)} %get-tuple-element.51, f32[8,4,64,128]{3,0,1,2:T(8,128)} %bitcast_multiply_fusion.8, f32[4,4,128,128]{3,2,1,0:T(8,128)} %all-gather.10.cloned.1.call-done, f32[4,4,128,128]{3,2,1,0:T(8,128)} %all-gather.8.cloned.1.call-done, ...), kind=kOutput, calls=%fused_computation.84 | convolution fusion | flops 405469184 | bytes 5799946 | tf_op jit(solution)/shard_map/gwme,wej->gwmj/dot_general | solution.py:181
  197.9 4.0 %all-to-all-start = ((bf16[4,128,512]{1,2,0:T(8,128)(2,1)}), bf16[4,128,512]{1,2,0:T(8,128)(2,1)S(1)}, u32[]{:S(2)}, u32[]{:S(2)}) async-start(bf16[4,128,512]{1,2,0:T(8,128)(2,1)} %copy.103), calls=%async_computation | async-start | bytes 1048576 | tf_op jit(solution)/shard_map/all_to_all | solution.py:185
  202.2 6.6 %all-to-all-done = bf16[4,128,512]{1,2,0:T(8,128)(2,1)S(1)} async-done(((bf16[4,128,512]{1,2,0:T(8,128)(2,1)}), bf16[4,128,512]{1,2,0:T(8,128)(2,1)S(1)}, u32[]{:S(2)}, u32[]{:S(2)}) %all-to-all-start) | async-done | bytes 524320 | tf_op jit(solution)/shard_map/all_to_all | solution.py:185
  208.8 4.8 %multiply_reduce_fusion = (f32[128]{0:T(128)S(1)}, f32[128,2048]{1,0:T(8,128)S(1)}) fusion(bf16[128,2048]{0,1:T(8,128)(2,1)S(1)} %bitcast.359, bf16[2048,2048]{1,0:T(8,128)(2,1)} %param.25, bf16[128,2048]{1,0:T(8,128)(2,1)S(1)} %copy-done.5), kind=kOutput, calls=%fused_computation.82 | convolution fusion | flops 1075314560 | bytes 10486272 | tf_op jit(solution)/shard_map/dot_general | solution.py:186
  214.3 2.2 reshape_transpose_transpose_reshape_reshape_reshape.3
  216.6 40.9 %all_to_all.29 = bf16[128,1,1,1,4,2048]{5,4,3,2,1,0:T(4,128)(2,1)S(1)} all-to-all(bf16[128,1,1,1,4,2048]{5,4,3,2,1,0:T(4,128)(2,1)} %bitcast.355), channel_id=1, replica_groups=mesh['sp_0'=4,'sp_1'=4,'sp_2'=2,'tp'=4] {'sp_0','sp_1','sp_2','tp'}, dimensions={0} | all-to-all | bytes 4194304 | tf_op jit(solution)/shard_map/all_to_all | solution.py:55
  257.5 4.7 %fusion.20 = f32[32,4,4,1024]{3,0,2,1:T(8,128)} fusion(bf16[1,2048,1024]{2,1,0:T(8,128)(2,1)S(1)} %copy-done.10, bf16[32,4,1,1,1,4,2048]{6,5,1,0,4,3,2:T(4,128)(2,1)S(1)} %bitcast.363), kind=kOutput, calls=%fused_computation.33 | convolution fusion | flops 2147483648 | bytes 8388608 | tf_op jit(solution)/shard_map/...ecd,edf->...ecf/dot_general | solution.py:143
  262.2 10.6 %fusion.27 = bf16[32,4,1,4,2048]{4,0,3,1,2:T(8,128)(2,1)} fusion(bf16[1,1024,2048]{2,1,0:T(8,128)(2,1)} %param.31, f32[32,4,4,1024]{3,0,2,1:T(8,128)} %fusion.20, bf16[1,2048,1024]{2,1,0:T(8,128)(2,1)} %param.29, bf16[32,4,1,1,1,4,2048]{6,5,1,0,4,3,2:T(4,128)(2,1)S(1)} %bitcast.364), kind=kOutput, calls=%fused_computation.39 | convolution fusion | flops 4299161600 | bytes 14680064 | tf_op jit(solution)/shard_map/...ecf,efd->...ecd/dot_general | solution.py:147
  272.8 4.5 %copy.111 = bf16[32,4,1,4,2048]{4,3,1,0,2:T(4,128)(2,1)} copy(bf16[32,4,1,4,2048]{4,0,3,1,2:T(8,128)(2,1)} %fusion.27) | data formatting | bytes 4194304 | tf_op jit(solution)/shard_map/convert_element_type | solution.py:149
  277.3 3.9 %all-to-all-start.2 = ((bf16[128,1,1,1,4,2048]{5,4,3,2,1,0:T(4,128)(2,1)}), bf16[128,1,1,1,4,2048]{5,4,3,2,1,0:T(4,128)(2,1)S(1)}, u32[]{:S(2)}, u32[]{:S(2)}) async-start(bf16[128,1,1,1,4,2048]{5,4,3,2,1,0:T(4,128)(2,1)} %bitcast.354), calls=%async_computation.2 | async-start | bytes 4194304 | tf_op jit(solution)/shard_map/all_to_all | solution.py:55
  281.4 30.7 %all-to-all-done.2 = bf16[128,1,1,1,4,2048]{5,4,3,2,1,0:T(4,128)(2,1)S(1)} async-done(((bf16[128,1,1,1,4,2048]{5,4,3,2,1,0:T(4,128)(2,1)}), bf16[128,1,1,1,4,2048]{5,4,3,2,1,0:T(4,128)(2,1)S(1)}, u32[]{:S(2)}, u32[]{:S(2)}) %all-to-all-start.2) | async-done | bytes 2097184 | tf_op jit(solution)/shard_map/all_to_all | solution.py:55
  313.5 2.5 reshape_reshape.3
  (152 shorter events, 41.7 us)
Async XLA Ops:
  6.5 157.1 %all-gather.8.cloned.1.call-start = ((), (), s32[]{:S(2)}) async-start(), calls=%async_computation.3 | async-start | bytes 1310720 | tf_op jit(solution)/shard_map/all_gather | solution.py:27
  10.6 2.7 copy-start.1
  12.0 2.7 copy-start.2
  14.7 1.7 copy-start.3
  133.3 32.7 %copy-start.7 = (s32[128,2]{0,1:T(2,128)S(1)}, s32[128,2]{0,1:T(2,128)}, u32[]{:S(2)}) copy-start(s32[128,2]{0,1:T(2,128)} %param.27) | copy-start | bytes 3076
  139.3 51.4 %all-gather.10.cloned.1.call-start = ((), (), s32[]{:S(2)}) async-start(), calls=%async_computation.4 | async-start | bytes 1310720 | tf_op jit(solution)/shard_map/all_gather | solution.py:27
  195.4 1.1 copy-start.4
  195.5 1.1 copy-start.8
  196.5 12.3 %copy-start.5 = (bf16[128,2048]{1,0:T(8,128)(2,1)S(1)}, bf16[128,2048]{1,0:T(8,128)(2,1)}, u32[]{:S(2)}) copy-start(bf16[128,2048]{1,0:T(8,128)(2,1)} %param.17) | copy-start | bytes 1572868
  197.9 10.9 %all-to-all-start = ((bf16[4,128,512]{1,2,0:T(8,128)(2,1)}), bf16[4,128,512]{1,2,0:T(8,128)(2,1)S(1)}, u32[]{:S(2)}, u32[]{:S(2)}) async-start(bf16[4,128,512]{1,2,0:T(8,128)(2,1)} %copy.103), calls=%async_computation | async-start | bytes 1048576 | tf_op jit(solution)/shard_map/all_to_all | solution.py:185
  208.8 4.8 %copy-start.6 = (f32[2048]{0:T(1024)S(1)}, f32[2048]{0:T(1024)}, u32[]{:S(2)}) copy-start(f32[2048]{0:T(1024)} %param.26) | copy-start | bytes 24580
  216.6 40.9 %copy-start.10 = (bf16[1,2048,1024]{2,1,0:T(8,128)(2,1)S(1)}, bf16[1,2048,1024]{2,1,0:T(8,128)(2,1)}, u32[]{:S(2)}) copy-start(bf16[1,2048,1024]{2,1,0:T(8,128)(2,1)} %param.30) | copy-start | bytes 12582916
  277.3 3.9 %copy-start.9 = (f32[128,2]{0,1:T(2,128)S(1)}, f32[128,2]{0,1:T(2,128)}, u32[]{:S(2)}) copy-start(f32[128,2]{0,1:T(2,128)} %param.28) | copy-start | bytes 3076
  277.3 34.8 %all-to-all-start.2 = ((bf16[128,1,1,1,4,2048]{5,4,3,2,1,0:T(4,128)(2,1)}), bf16[128,1,1,1,4,2048]{5,4,3,2,1,0:T(4,128)(2,1)S(1)}, u32[]{:S(2)}, u32[]{:S(2)}) async-start(bf16[128,1,1,1,4,2048]{5,4,3,2,1,0:T(4,128)(2,1)} %bitcast.354), calls=%async_computation.2 | async-start | bytes 4194304 | tf_op jit(solution)/shard_map/all_to_all | solution.py:55
  312.1 1.3 copy-start
Sparse Core Ops, SparseCore 0:
  139.4 24.1 all-gather.7
  166.0 24.6 all-gather.9
where the time goes:
time: 326 us; the launch traced here: 325 us
  other arithmetic  83.9 us (26%)
  waiting for transfers between devices  66.1 us (20%)
  blocking collectives  63.6 us (20%)
  matrix products  51.1 us (16%)
  local copies, waits for them, and re-layouts  37.7 us (12%)
  between operations  13.7 us (4%)
  starting transfers between devices  7.93 us (2%)
    dot_general x8, other arithmetic, advance(): jnp.einsum('htk,hsk,htsk->hts', query_block, key_b, weight_t, precision=m...  58.6 us
    all_to_all x1, blocking collectives, one_exchange(): parts = lax.all_to_all(parts, axis, split_axis=0, concat_axis=0, tiled=True)  40.9 us
    all_to_all x1, waiting for transfers between devices, one_exchange(): parts = lax.all_to_all(parts, axis, split_axis=0, concat_axis=0, tiled=True)  30.7 us
    all_gather x2, waiting for transfers between devices, carried_in(): pieces = jax.tree.map(lambda part: lax.all_gather(part, axis), so_far)  28.8 us
    all_gather x4, blocking collectives, carried_in(): pieces = jax.tree.map(lambda part: lax.all_gather(part, axis), so_far)  22.7 us
    dot_general x8, matrix products, advance(): jnp.einsum('bup,bpl->bul', query_block * jnp.exp(cumulative_block), curre...  15.4 us
    select_n x8, other arithmetic, advance(): weight_t = jnp.where(causal, jnp.exp(jnp.where(causal, spread, 0.0)), 0.0)  13.6 us
    dot_general x1, matrix products, expert_block(): jnp.einsum('...ecf,efd->...ecd', hidden, down_matrix, preferred_element_t...  10.6 us
  transfers between devices with their start and end apart: 4, of which 4 were waited for; matrix products, arithmetic and copies ran while one was open for 1% of the time, Pallas kernels for 0%

commit v1 on v0

--- a/solution.py
+++ b/solution.py
@@ -1,6 +1,10 @@
+import functools
+
 import jax
 import jax.numpy as jnp
 from jax import lax
+from jax.experimental import pallas as pl
+from jax.experimental.pallas import tpu as pltpu
 from jax.sharding import Mesh
 from jax.sharding import PartitionSpec as P
 
@@ -149,6 +153,229 @@
     ).astype(jnp.bfloat16)
 
 
+MESH = pl.DeviceIdType.MESH
+F32 = jnp.float32
+BF16 = jnp.bfloat16
+I32 = jnp.int32
+GROUPS = 4
+PER = 32
+
+
+def coords():
+    sp = lax.axis_index("sp")
+    return sp // 8, (sp // 2) % 4, sp % 2, lax.axis_index("tp")
+
+
+def peer(d, sign):
+    z, y, c, x = coords()
+    g, j = d // PER, d % PER
+    dz, dy, dc = j // 8, (j // 2) % 4, j % 2
+    dx = (g + 8 - dz - dy) % 4
+    if sign < 0:
+        dz, dy, dx = 4 - dz, 4 - dy, 4 - dx
+    z, y, c, x = (z + dz) % 4, (y + dy) % 4, (c + dc) % 2, (x + dx) % 4
+    return ((z * 4 + y) * 2 + c, x)
+
+
+def entry_barrier():
+    barrier = pltpu.get_barrier_semaphore()
+
+    @pl.loop(1, GROUPS * PER)
+    def _(d):
+        pl.semaphore_signal(barrier, inc=1, device_id=peer(d, 1), device_id_type=MESH)
+
+    return barrier
+
+
+def iota(shape, dim):
+    return lax.broadcasted_iota(I32, shape, dim)
+
+
+def slot_tables(routes, weights, pack_l, comb_l):
+    z, y, c, x = coords()
+    d = iota((128, 128), 0)
+    dz, dy, dc = (d >> 3) & 3, (d >> 1) & 3, d & 1
+    dx = ((d >> 5) + 8 - dz - dy) & 3
+    expert = (((((z + dz) & 3) * 4 + ((y + dy) & 3)) * 2 + ((c + dc) & 1)) * 4) + ((x + dx) & 3)
+    first = routes[0:1, :] == expert
+    second = routes[1:2, :] == expert
+    member = jnp.where(first, 1.0, jnp.where(second, 1.0, 0.0))
+    earlier = jnp.where(iota((128, 128), 0) < iota((128, 128), 1), 1.0, 0.0).astype(BF16)
+    rank = jnp.dot(member.astype(BF16), earlier, preferred_element_type=F32)
+    code = (member * (rank + 1.0)).astype(BF16)
+    share = jnp.where(first, weights[0:1, :], jnp.where(second, weights[1:2, :], 0.0))
+    high = share.astype(BF16)
+    low = (share - high.astype(F32)).astype(BF16)
+    table = jnp.concatenate([code, high, low], axis=1)
+    rows = PER * 8
+    at = iota((rows, 128), 0)
+    wanted = ((at & 3) + 1).astype(F32)
+    upper = ((at >> 2) & 1) == 0
+    for g in range(GROUPS):
+        spread = jnp.where((at >> 3) + g * PER == iota((rows, 128), 1), 1.0, 0.0).astype(BF16)
+        wide = jnp.dot(spread, table, preferred_element_type=F32)
+        chosen = wide[:, :128] == wanted
+        one = jnp.where(chosen, 1.0, 0.0)
+        high_g = jnp.where(chosen, wide[:, 128:256], 0.0)
+        low_g = jnp.where(chosen, wide[:, 256:], 0.0)
+        zero = jnp.zeros_like(one)
+        pack_l[g] = jnp.concatenate(
+            [jnp.where(upper, one, zero), jnp.where(upper, zero, one)], axis=1
+        ).astype(BF16)
+        comb_l[g] = jnp.concatenate(
+            [
+                jnp.where(upper, high_g, zero),
+                jnp.where(upper, zero, high_g),
+                jnp.where(upper, low_g, zero),
+                jnp.where(upper, zero, low_g),
+            ],
+            axis=1,
+        ).astype(BF16)
+
+
+def blocks(ref, lo, count):
+    return ref.at[pl.ds(lo, count)]
+
+
+def wait_group(buf, sem, g):
+    z, y, c, x = coords()
+    other = (lax.axis_index("sp"), (x + 1) % 4)
+
+    @pl.when(g == 0)
+    def _():
+        part = blocks(buf, 1, PER - 1)
+        pltpu.make_async_remote_copy(part, part, sem, sem, other, MESH).wait_recv()
+
+    @pl.when(g > 0)
+    def _():
+        part = blocks(buf, g * PER, PER)
+        pltpu.make_async_remote_copy(part, part, sem, sem, other, MESH).wait_recv()
+
+
+def send_group(src, dst, send_sem, recv_sem, g, sign):
+    @pl.loop(0, PER)
+    def _(j):
+        d = g * PER + j
+
+        @pl.when(d > 0)
+        def _():
+            pltpu.make_async_remote_copy(
+                src.at[d], dst.at[d], send_sem, recv_sem, peer(d, sign), MESH
+            ).start()
+
+
+def wait_sent(buf, sem):
+    x = lax.axis_index("tp")
+    part = blocks(buf, 1, GROUPS * PER - 1)
+    pltpu.make_async_remote_copy(
+        part, part, sem, sem, (lax.axis_index("sp"), (x + 1) % 4), MESH
+    ).wait_send()
+
+
+def expert_phase(stream, normed, pack_l, comb_l, gate, up, down, weight_copies, bufs, total, out):
+    out_slots, in_slots, answers, replies, send_sem, recv_sem, send_back, recv_back = bufs
+    halves = jnp.concatenate([normed[:, :1024], normed[:, 1024:]], axis=0)
+    for g in range(GROUPS):
+        packed = jnp.dot(pack_l[g], halves, preferred_element_type=F32).astype(BF16)
+        out_slots[pl.ds(g * PER, PER)] = packed.reshape(PER, 8, 1024)
+        send_group(out_slots, in_slots, send_sem, recv_sem.at[g], g, 1)
+    in_slots[0] = out_slots[0]
+    for copy in weight_copies:
+        copy.wait()
+    rows = PER * 8
+    a, b = iota((rows, rows), 0), iota((rows, rows), 1)
+    place = ((a & 127) >> 2) * 8 + (a >> 7) * 4 + (a & 3)
+    unpack = jnp.where(place == b, 1.0, 0.0).astype(BF16)
+    place_b = ((b & 127) >> 2) * 8 + (b >> 7) * 4 + (b & 3)
+    repack = jnp.where(place_b == a, 1.0, 0.0).astype(BF16)
+
+    @pl.loop(0, GROUPS)
+    def _(g):
+        wait_group(in_slots, recv_sem.at[g], g)
+        came = in_slots[pl.ds(g * PER, PER)].reshape(rows, 1024)
+        flat = jnp.dot(unpack, came, preferred_element_type=F32).astype(BF16)
+        x = jnp.concatenate([flat[:128], flat[128:]], axis=1)
+        hidden = []
+        for n in range(0, 1024, 256):
+            gated = jnp.dot(x, gate[:, n : n + 256], preferred_element_type=F32)
+            lifted = jnp.dot(x, up[:, n : n + 256], preferred_element_type=F32)
+            hidden.append((gated * jax.nn.sigmoid(gated) * lifted).astype(BF16))
+        hidden = jnp.concatenate(hidden, axis=1)
+        y0 = jnp.dot(hidden, down[:, :1024], preferred_element_type=F32).astype(BF16)
+        y1 = jnp.dot(hidden, down[:, 1024:], preferred_element_type=F32).astype(BF16)
+        both = jnp.concatenate([y0, y1], axis=0)
+        back = jnp.dot(repack, both, preferred_element_type=F32).astype(BF16)
+        answers[pl.ds(g * PER, PER)] = back.reshape(PER, 8, 1024)
+        send_group(answers, replies, send_back, recv_back.at[g], g, -1)
+
+    replies[0] = answers[0]
+    total[...] = jnp.zeros_like(total)
+
+    @pl.loop(0, GROUPS)
+    def _(g):
+        wait_group(replies, recv_back.at[g], g)
+        got = replies[pl.ds(g * PER, PER)].reshape(rows, 1024)
+        total[...] += lax.dot_general(
+            comb_l[g], got, (((0,), (0,)), ((), ())), preferred_element_type=F32
+        )
+
+    for h in range(2):
+        part = total[h * 128 : h * 128 + 128] + total[256 + h * 128 : 256 + h * 128 + 128]
+        cols = slice(h * 1024, h * 1024 + 1024)
+        out[:, cols] = (stream[:, cols].astype(F32) + part).astype(BF16)
+    wait_sent(out_slots, send_sem)
+    wait_sent(answers, send_back)
+
+
+def slot_buffers():
+    slots = pltpu.VMEM((GROUPS * PER, 8, 1024), BF16)
+    dma = pltpu.SemaphoreType.DMA
+    return [slots] * 4 + [dma, dma((GROUPS,)), dma, dma((GROUPS,))]
+
+
+def expert_kernel(
+    stream, scale, routes, weights, gate_hbm, up_hbm, down_hbm, out,
+    gate, up, down, w_sems, pack_l, comb_l, total, *bufs,
+):
+    barrier = entry_barrier()
+    copies = [
+        pltpu.make_async_copy(src.at[0], dst, w_sems.at[i])
+        for i, (src, dst) in enumerate(((gate_hbm, gate), (up_hbm, up), (down_hbm, down)))
+    ]
+    for copy in copies:
+        copy.start()
+    slot_tables(routes, weights, pack_l, comb_l)
+    values = stream[...].astype(F32)
+    square = jnp.mean(values * values, axis=1, keepdims=True)
+    normed = (values * lax.rsqrt(square + 1e-06) * scale[...]).astype(BF16)
+    pl.semaphore_wait(barrier, GROUPS * PER - 1)
+    expert_phase(stream, normed, pack_l, comb_l, gate, up, down, copies, bufs, total, out)
+
+
+def expert_call(stream, scale, routes, weights, gate, up, down):
+    vmem = pl.BlockSpec(memory_space=pltpu.VMEM)
+    hbm = pl.BlockSpec(memory_space=pl.ANY)
+    return pl.pallas_call(
+        expert_kernel,
+        out_shape=jax.ShapeDtypeStruct((128, 2048), BF16),
+        in_specs=[vmem] * 4 + [hbm] * 3,
+        out_specs=vmem,
+        scratch_shapes=[
+            pltpu.VMEM((2048, 1024), BF16),
+            pltpu.VMEM((2048, 1024), BF16),
+            pltpu.VMEM((1024, 2048), BF16),
+            pltpu.SemaphoreType.DMA((3,)),
+            pltpu.VMEM((GROUPS, PER * 8, 256), BF16),
+            pltpu.VMEM((GROUPS, PER * 8, 512), BF16),
+            pltpu.VMEM((512, 1024), F32),
+        ]
+        + slot_buffers(),
+        compiler_params=pltpu.CompilerParams(
+            collective_id=0, has_side_effects=True, vmem_limit_bytes=60 * 1024 * 1024
+        ),
+    )(stream, scale.reshape(1, 2048), routes.T, weights.T, gate, up, down)
+
+
 def body(
     resid,
     query,
@@ -185,42 +412,7 @@
     arrived_rows = lax.all_to_all(gated_rows, "tp", split_axis=0, concat_axis=1, tiled=True)
     mixed_rows = jnp.dot(arrived_rows, output_matrix, preferred_element_type=jnp.float32)
     stream = (resid.astype(jnp.float32) + mixed_rows).astype(jnp.bfloat16)
-    normed = row_norm(stream, norm_scale_vector)
-    row_count = routes.shape[0]
-    top_count = routes.shape[1]
-    model_width = normed.shape[1]
-    per_device = gate_matrix.shape[0]
-    devices = lax.axis_size(SP) * lax.axis_size("tp")
-    experts = per_device * devices
-    capacity = 2 * row_count * top_count // experts
-    flat_routes = routes.reshape(-1)
-    member = (flat_routes[:, None] == jnp.arange(experts, dtype=jnp.int32)[None, :]).astype(
-        jnp.int32
-    )
-    slot_rank = jnp.sum(jnp.cumsum(member, axis=0) * member, axis=1) - 1
-    position_entries = flat_routes * capacity + slot_rank
-    select = (
-        position_entries[:, None] == jnp.arange(experts * capacity, dtype=jnp.int32)[None, :]
-    ).astype(jnp.bfloat16)
-    select = select.reshape(row_count, top_count, experts * capacity)
-    dispatch = jnp.sum(select, axis=1)
-    packed = lax.dot_general(
-        dispatch, normed, (((0,), (0,)), ((), ())), preferred_element_type=jnp.float32
-    ).astype(jnp.bfloat16)
-    sectioned = packed.reshape(
-        lax.axis_size(SP), lax.axis_size("tp"), per_device, capacity, model_width
-    )
-    arrived = one_exchange(sectioned, SP_TP, (SP, "tp"), (0, 1), (0, 1))
-    answers = expert_block(arrived, gate_matrix, up_matrix, down_matrix)
-    returned = one_exchange(answers, SP_TP, (SP, "tp"), (0, 1), (0, 1))
-    returned_rows = returned.reshape(experts * capacity, model_width)
-    combined = stream.astype(jnp.float32)
-    for pick_index in range(top_count):
-        picked = jnp.dot(
-            select[:, pick_index, :], returned_rows, preferred_element_type=jnp.float32
-        )
-        combined = combined + routing_weight[:, pick_index : pick_index + 1] * picked
-    return combined.astype(jnp.bfloat16)
+    return stream
 
 
 def solution(mesh):
@@ -242,6 +434,19 @@
         P(SP_TP, None, None),
         P(SP_TP, None, None),
     )
-    return jax.shard_map(
+    front = jax.shard_map(
         body, mesh=finer, in_specs=placed, out_specs=P(SP_TP, None), check_vma=False
     )
+    whole = ("sp", "tp")
+    back = jax.shard_map(
+        expert_call,
+        mesh=mesh,
+        in_specs=(P(whole, None), P(), P(whole, None), P(whole, None)) + (P(whole, None, None),) * 3,
+        out_specs=P(whole, None),
+        check_vma=False,
+    )
+
+    def run(*args):
+        return back(front(*args), args[9], *args[10:])
+
+    return run

time: 326 us -> 291 us (0.89)
  Pallas kernels: 0 us -> 78.8 us
  waiting for transfers between devices: 66.1 us -> 29.8 us
  blocking collectives: 63.6 us -> 33.5 us
  matrix products: 51.1 us -> 26.7 us
  local copies, waits for them, and re-layouts: 37.7 us -> 22.1 us
  starting transfers between devices: 7.93 us -> 0.04 us
    pallas_call x0 -> x1, Pallas kernels: none -> 78.8 us  [expert_call(): pl.pallas_call(expert_kernel, out_shape=jax.ShapeDtypeStruct((128, 2048),...]
    all_to_all x2 -> x0, waiting for transfers between devices: 37.3 us -> none  [the longest x1 30.7 us: one_exchange(): parts = lax.all_to_all(parts, axis, split_axis=0, concat_axis=0, tiled=True)]
    all_to_all x1, blocking collectives: 40.9 us -> 10.7 us  [body(): lax.all_to_all(gated_rows, 'tp', split_axis=0, concat_axis=1, tiled=True)]
    dot_general x5 -> x0, matrix products: 17.8 us -> none  [the longest x1 10.6 us: expert_block(): jnp.einsum('...ecf,efd->...ecd', hidden, down_matrix, preferred_element_t...]
    all_to_all x2 -> x0, starting transfers between devices: 7.89 us -> none  [the longest x1 3.97 us: body(): lax.all_to_all(gated_rows, 'tp', split_axis=0, concat_axis=1, tiled=True)]
    dot_general x8, matrix products: 15.4 us -> 8.18 us  [advance(): jnp.einsum('bup,bpl->bul', query_block * jnp.exp(cumulative_block), curre...]
    squeeze x8, local copies, waits for them, and re-layouts: 7.36 us -> 0.14 us  [block_recurrence(): lax.scan(advance, start_state, (queries, keys_in, values, cum_log))]
    another operation x5 -> x0, local copies, waits for them, and re-layouts: 4.76 us -> none  [the longest x1 2.53 us: body(): returned_rows = returned.reshape(experts * capacity, model_width)]
  transfers between devices with their start and end apart: 4 -> 2, of which waited for: 4 -> 2; matrix products, arithmetic and copies ran while one was open for 1% -> 1% of each run, Pallas kernels for 0% -> 0%
where the time goes in v1:
time: 291 us; the launch traced here: 290 us
  other arithmetic  84.5 us (29%)
  Pallas kernels  78.8 us (27%)
  blocking collectives  33.5 us (12%)
  waiting for transfers between devices  29.8 us (10%)
  matrix products  26.7 us (9%)
  local copies, waits for them, and re-layouts  22.1 us (8%)
  between operations  13.6 us (5%)
    pallas_call x1, Pallas kernels, expert_call(): pl.pallas_call(expert_kernel, out_shape=jax.ShapeDtypeStruct((128, 2048),...  78.8 us
    dot_general x8, other arithmetic, advance(): jnp.einsum('htk,hsk,htsk->hts', query_block, key_b, weight_t, precision=m...  58.6 us
    all_gather x2, waiting for transfers between devices, carried_in(): pieces = jax.tree.map(lambda part: lax.all_gather(part, axis), so_far)  29.8 us
    all_gather x4, blocking collectives, carried_in(): pieces = jax.tree.map(lambda part: lax.all_gather(part, axis), so_far)  22.8 us
    select_n x8, other arithmetic, advance(): weight_t = jnp.where(causal, jnp.exp(jnp.where(causal, spread, 0.0)), 0.0)  13.6 us
    all_to_all x1, blocking collectives, body(): lax.all_to_all(gated_rows, 'tp', split_axis=0, concat_axis=1, tiled=True)  10.7 us
    dynamic_slice x32, local copies, waits for them, and re-layouts, block_recurrence(): lax.scan(advance, start_state, (queries, keys_in, values, cum_log))  9.04 us
    dot_general x8, matrix products, advance(): jnp.einsum('bup,bpl->bul', query_block * jnp.exp(cumulative_block), curre...  8.18 us
  transfers between devices with their start and end apart: 2, of which 2 were waited for; matrix products, arithmetic and copies ran while one was open for 1% of the time, Pallas kernels for 0%

profile of v1, /device:TPU:1, one launch (start us, length us, event | category | flops | bytes accessed | tf_op | source)
XLA Modules:
  0.0 290.0 jit_solution(12896874285930651092)
XLA Ops:
  6.5 1.6 copy.52
  8.1 1.2 convert_multiply_fusion.2
  9.8 1.3 convert_multiply_fusion.1
  11.1 1.3 reshape.200
  12.4 1.5 broadcast_in_dim.32
  14.0 3.0 %divide_multiply_fusion = (f32[512,512]{1,0:T(8,128)}, f32[512,512]{1,0:T(8,128)}) fusion(bf16[512,512]{1,0:T(8,128)(2,1)} %param.20, f32[512]{0:T(512)S(1)} %copy-done.2, f32[64,8,4,128]{3,2,1,0:T(4,128)S(1)} %bitcast.228), kind=kLoop, calls=%fused_computation.57 | loop fusion | flops 1572864 | bytes 3672064 | tf_op jit(solution)/shard_map/mul | solution.py:78
  17.0 2.6 reshape.199
  19.5 2.5 reshape.198
  22.1 1.3 fusion.27
  23.4 98.9 %while.14 = (s32[]{:T(128)}, f32[4,128,128]{2,1,0:T(8,128)S(1)}, f32[8,4,64,128]{3,2,0,1:T(8,128)}, f32[8,4,64,128]{3,0,1,2:T(8,128)S(1)}, f32[8,4,64,128]{3,1,2...) while((s32[]{:T(128)}, f32[4,128,128]{2,1,0:T(8,128)S(1)}, ...), condition=%wide.region_2.3_spmd.clone.clone, body=%wide.region_1.2_spmd.clone.clone.sunk | while | flops 138792960 | bytes 20862588 | solution.py:121
  23.8 1.0 constant_dynamic-slice_fusion.6
  24.8 1.7 exponential_select_fusion.2
  26.5 7.3 %fusion.117 = f32[4,64,64]{1,2,0:T(8,128)S(1)} fusion(f32[4,64,64,128]{3,2,1,0:T(8,128)S(1)} %exponential_select_fusion.2, f32[4,128,64]{1,2,0:T(8,128)S(1)} %dynamic-slice_bitcast_fusion.2, f32[4,128,64]{1,2,0:T(8,128)S(1)} %bitcast.226), kind=kLoop, calls=%fused_computation.2.clone.1 | loop fusion | flops 6275072 | bytes 8716288 | tf_op jit(solution)/shard_map/while/body/eval_jaxpr/htk,hsk,htsk->hts/dot_general | solution.py:103
  34.2 1.0 fusion.119
  37.1 1.7 exponential_select_fusion.2
  38.8 7.3 %fusion.117 = f32[4,64,64]{1,2,0:T(8,128)S(1)} fusion(f32[4,64,64,128]{3,2,1,0:T(8,128)S(1)} %exponential_select_fusion.2, f32[4,128,64]{1,2,0:T(8,128)S(1)} %dynamic-slice_bitcast_fusion.2, f32[4,128,64]{1,2,0:T(8,128)S(1)} %bitcast.226), kind=kLoop, calls=%fused_computation.2.clone.1 | loop fusion | flops 6275072 | bytes 8716288 | tf_op jit(solution)/shard_map/while/body/eval_jaxpr/htk,hsk,htsk->hts/dot_general | solution.py:103
  46.6 1.0 fusion.119
  49.5 1.7 exponential_select_fusion.2
  51.2 7.3 %fusion.117 = f32[4,64,64]{1,2,0:T(8,128)S(1)} fusion(f32[4,64,64,128]{3,2,1,0:T(8,128)S(1)} %exponential_select_fusion.2, f32[4,128,64]{1,2,0:T(8,128)S(1)} %dynamic-slice_bitcast_fusion.2, f32[4,128,64]{1,2,0:T(8,128)S(1)} %bitcast.226), kind=kLoop, calls=%fused_computation.2.clone.1 | loop fusion | flops 6275072 | bytes 8716288 | tf_op jit(solution)/shard_map/while/body/eval_jaxpr/htk,hsk,htsk->hts/dot_general | solution.py:103
  58.9 1.0 fusion.119
  61.8 1.7 exponential_select_fusion.2
  63.5 7.3 %fusion.117 = f32[4,64,64]{1,2,0:T(8,128)S(1)} fusion(f32[4,64,64,128]{3,2,1,0:T(8,128)S(1)} %exponential_select_fusion.2, f32[4,128,64]{1,2,0:T(8,128)S(1)} %dynamic-slice_bitcast_fusion.2, f32[4,128,64]{1,2,0:T(8,128)S(1)} %bitcast.226), kind=kLoop, calls=%fused_computation.2.clone.1 | loop fusion | flops 6275072 | bytes 8716288 | tf_op jit(solution)/shard_map/while/body/eval_jaxpr/htk,hsk,htsk->hts/dot_general | solution.py:103
  71.2 1.0 fusion.119
  74.2 1.7 exponential_select_fusion.2
  75.9 7.3 %fusion.117 = f32[4,64,64]{1,2,0:T(8,128)S(1)} fusion(f32[4,64,64,128]{3,2,1,0:T(8,128)S(1)} %exponential_select_fusion.2, f32[4,128,64]{1,2,0:T(8,128)S(1)} %dynamic-slice_bitcast_fusion.2, f32[4,128,64]{1,2,0:T(8,128)S(1)} %bitcast.226), kind=kLoop, calls=%fused_computation.2.clone.1 | loop fusion | flops 6275072 | bytes 8716288 | tf_op jit(solution)/shard_map/while/body/eval_jaxpr/htk,hsk,htsk->hts/dot_general | solution.py:103
  83.6 1.0 fusion.119
  86.5 1.7 exponential_select_fusion.2
  88.2 7.3 %fusion.117 = f32[4,64,64]{1,2,0:T(8,128)S(1)} fusion(f32[4,64,64,128]{3,2,1,0:T(8,128)S(1)} %exponential_select_fusion.2, f32[4,128,64]{1,2,0:T(8,128)S(1)} %dynamic-slice_bitcast_fusion.2, f32[4,128,64]{1,2,0:T(8,128)S(1)} %bitcast.226), kind=kLoop, calls=%fused_computation.2.clone.1 | loop fusion | flops 6275072 | bytes 8716288 | tf_op jit(solution)/shard_map/while/body/eval_jaxpr/htk,hsk,htsk->hts/dot_general | solution.py:103
  95.9 1.0 fusion.119
  98.9 1.7 exponential_select_fusion.2
  100.6 7.3 %fusion.117 = f32[4,64,64]{1,2,0:T(8,128)S(1)} fusion(f32[4,64,64,128]{3,2,1,0:T(8,128)S(1)} %exponential_select_fusion.2, f32[4,128,64]{1,2,0:T(8,128)S(1)} %dynamic-slice_bitcast_fusion.2, f32[4,128,64]{1,2,0:T(8,128)S(1)} %bitcast.226), kind=kLoop, calls=%fused_computation.2.clone.1 | loop fusion | flops 6275072 | bytes 8716288 | tf_op jit(solution)/shard_map/while/body/eval_jaxpr/htk,hsk,htsk->hts/dot_general | solution.py:103
  108.3 1.0 fusion.119
  111.2 1.7 exponential_select_fusion.2
  112.9 7.3 %fusion.117 = f32[4,64,64]{1,2,0:T(8,128)S(1)} fusion(f32[4,64,64,128]{3,2,1,0:T(8,128)S(1)} %exponential_select_fusion.2, f32[4,128,64]{1,2,0:T(8,128)S(1)} %dynamic-slice_bitcast_fusion.2, f32[4,128,64]{1,2,0:T(8,128)S(1)} %bitcast.226), kind=kLoop, calls=%fused_computation.2.clone.1 | loop fusion | flops 6275072 | bytes 8716288 | tf_op jit(solution)/shard_map/while/body/eval_jaxpr/htk,hsk,htsk->hts/dot_general | solution.py:103
  120.6 1.0 fusion.119
  122.4 3.0 %all-gather.3 = f32[2,4,128]{2,1,0:T(4,128)S(1)} all-gather(f32[1,4,128]{2,1,0:T(4,128)S(1)} %bitcast.237), channel_id=2, replica_groups=mesh['sp_0'=4,'sp_1'=4,'sp_2'=2,'tp'=4] {'sp_2'}, dimensions={0}, use_global_device_ids=true | all-gather | bytes 6144 | tf_op jit(solution)/shard_map/all_gather | solution.py:31
  125.4 2.2 all-gather.1
  128.6 8.8 %all-gather.4 = f32[4,4,128]{2,1,0:T(4,128)S(1)} all-gather(f32[1,4,128]{2,1,0:T(4,128)S(1)} %get-tuple-element.143), channel_id=4, replica_groups=mesh['sp_0'=4,'sp_1'=4,'sp_2'=2,'tp'=4] {'sp_1'}, dimensions={0}, use_global_device_ids=true | all-gather | bytes 10240 | tf_op jit(solution)/shard_map/all_gather | solution.py:31
  137.4 15.5 %all-gather.8.cloned.1.call-done = f32[4,4,128,128]{3,2,1,0:T(8,128)} async-done(((f32[1,4,128,128]{3,2,1,0:T(8,128)}), f32[4,4,128,128]{3,2,1,0:T(8,128)}) %all-gather.8.cloned.1.call-update) | async-done | bytes 1048592 | tf_op jit(solution)/shard_map/all_gather | solution.py:31
  152.9 2.2 multiply_add_fusion
  155.1 8.8 %all_gather.31 = f32[4,4,128]{2,1,0:T(4,128)S(1)} all-gather(f32[1,4,128]{2,1,0:T(4,128)S(1)} %get-tuple-element.151), channel_id=1, replica_groups=mesh['sp_0'=4,'sp_1'=4,'sp_2'=2,'tp'=4] {'sp_0'}, dimensions={0}, use_global_device_ids=true | all-gather | bytes 10240 | tf_op jit(solution)/shard_map/all_gather | solution.py:31
  164.0 1.6 bitcast_multiply_fusion.6
  165.6 14.3 %all-gather.10.cloned.1.call-done = f32[4,4,128,128]{3,2,1,0:T(8,128)} async-done(((f32[1,4,128,128]{3,2,1,0:T(8,128)}), f32[4,4,128,128]{3,2,1,0:T(8,128)}) %all-gather.10.cloned.1.call-update) | async-done | bytes 1048592 | tf_op jit(solution)/shard_map/all_gather | solution.py:31
  179.9 4.7 %multiply_reduce_fusion = (f32[8,4,64]{2,0,1:T(8,128)S(1)}, f32[8,4,64,128]{3,2,0,1:T(8,128)S(1)}) fusion(f32[8,4,64,128]{3,2,0,1:T(8,128)} %get-tuple-element.52, f32[8,4,64,128]{3,0,1,2:T(8,128)} %bitcast_multiply_fusion.6, f32[4,4,128,128]{3,2,1,0:T(8,128)} %all-gather.10.cloned.1.call-done, f32[4,4,128,128]{3,2,1,0:T(8,128)} %all-gather.8.cloned.1.call-done, ...), kind=kOutput, calls=%fused_computation.55 | convolution fusion | flops 405469184 | bytes 5799946 | tf_op jit(solution)/shard_map/gwme,wej->gwmj/dot_general | solution.py:408
  186.3 10.7 %all_to_all.19 = bf16[4,128,512]{1,2,0:T(8,128)(2,1)S(1)} all-to-all(bf16[4,128,512]{1,2,0:T(8,128)(2,1)S(1)} %copy.62), channel_id=1, replica_groups=mesh['sp_0'=4,'sp_1'=4,'sp_2'=2,'tp'=4] {'tp'}, dimensions={0} | all-to-all | bytes 1048576 | tf_op jit(solution)/shard_map/all_to_all | solution.py:412
  197.0 5.5 %fusion.18.stream = bf16[128,2048]{1,0:T(8,128)(2,1)} fusion(bf16[128,2048]{0,1:T(8,128)(2,1)S(1)} %bitcast.230, bf16[2048,2048]{1,0:T(8,128)(2,1)} %param.26, bf16[128,2048]{1,0:T(8,128)(2,1)S(1)} %copy-done.1), kind=kOutput, calls=%fused_computation.32 | convolution fusion | flops 1074528256 | bytes 9961472 | tf_op jit(solution)/shard_map/dot_general | solution.py:413
  202.5 78.8 %shard_map.164 = bf16[128,2048]{1,0:T(8,128)(2,1)} custom-call(bf16[128,2048]{1,0:T(8,128)(2,1)} %fusion.18.stream, f32[1,2048]{1,0:T(1,128)} %bitcast.236, s32[2,128]{1,0:T(2,128)} %bitcast.238, f32[2,128]{1,0:T(2,128)} %bitcast.239, bf16[1,2048,1024]{2,1,0:T(8,128)(2,1)} %gate_hbm.1, bf16[1,2048,1024]{2,1,0:T(8,128)(2,1)} %up_hbm.1, ...), custom_call_target="tpu_custom_call" | custom-call | tf_op jit(solution)/shard_map/pallas_call | solution.py:358
  281.3 1.9 copy.143
  (108 shorter events, 19.9 us)
Async XLA Ops:
  6.5 7.4 %copy-start.2 = (f32[512]{0:T(512)S(1)}, f32[512]{0:T(512)}, u32[]{:S(2)}) copy-start(f32[512]{0:T(512)} %param.21) | copy-start | bytes 6148
  6.5 146.3 %all-gather.8.cloned.1.call-start = ((), (), s32[]{:S(2)}) async-start(), calls=%async_computation.1 | async-start | bytes 1310720 | tf_op jit(solution)/shard_map/all_gather | solution.py:31
  122.3 63.4 %copy-start = (bf16[512,512]{1,0:T(8,128)(2,1)S(1)}, bf16[512,512]{1,0:T(8,128)(2,1)}, u32[]{:S(2)}) copy-start(bf16[512,512]{1,0:T(8,128)(2,1)} %param.24) | copy-start | bytes 1572868
  122.3 63.4 %copy-start.3 = (f32[512]{0:T(512)S(1)}, f32[512]{0:T(512)}, u32[]{:S(2)}) copy-start(f32[512]{0:T(512)} %param.25) | copy-start | bytes 6148
  128.5 51.4 %all-gather.10.cloned.1.call-start = ((), (), s32[]{:S(2)}) async-start(), calls=%async_computation.2 | async-start | bytes 1310720 | tf_op jit(solution)/shard_map/all_gather | solution.py:31
  184.6 12.4 %copy-start.1 = (bf16[128,2048]{1,0:T(8,128)(2,1)S(1)}, bf16[128,2048]{1,0:T(8,128)(2,1)}, u32[]{:S(2)}) copy-start(bf16[128,2048]{1,0:T(8,128)(2,1)} %param.18) | copy-start | bytes 1572868
Sparse Core Ops, SparseCore 0:
  128.6 24.1 all-gather.7
  155.2 24.6 all-gather.9

commit v2 on v1

v2 whole, which is shorter than its diff:
```python
import jax
import jax.numpy as jnp
from jax import lax
from jax.experimental import pallas as pl
from jax.experimental.pallas import tpu as pltpu
from jax.sharding import PartitionSpec as P

MESH = pl.DeviceIdType.MESH
F32 = jnp.float32
BF16 = jnp.bfloat16
I32 = jnp.int32
GROUPS = 4
PER = 32


def coords():
    sp = lax.axis_index("sp")
    return sp // 8, (sp // 2) % 4, sp % 2, lax.axis_index("tp")


def peer(d, sign):
    z, y, c, x = coords()
    g, j = d // PER, d % PER
    dz, dy, dc = j // 8, (j // 2) % 4, j % 2
    dx = (g + 8 - dz - dy) % 4
    if sign < 0:
        dz, dy, dx = 4 - dz, 4 - dy, 4 - dx
    z, y, c, x = (z + dz) % 4, (y + dy) % 4, (c + dc) % 2, (x + dx) % 4
    return ((z * 4 + y) * 2 + c, x)


def entry_barrier():
    barrier = pltpu.get_barrier_semaphore()

    @pl.loop(1, GROUPS * PER)
    def _(d):
        pl.semaphore_signal(barrier, inc=1, device_id=peer(d, 1), device_id_type=MESH)

    return barrier


def iota(shape, dim):
    return lax.broadcasted_iota(I32, shape, dim)


def slot_tables(routes, weights, pack_l, comb_l):
    z, y, c, x = coords()
    d = iota((128, 128), 0)
    dz, dy, dc = (d >> 3) & 3, (d >> 1) & 3, d & 1
    dx = ((d >> 5) + 8 - dz - dy) & 3
    expert = (((((z + dz) & 3) * 4 + ((y + dy) & 3)) * 2 + ((c + dc) & 1)) * 4) + ((x + dx) & 3)
    first = routes[0:1, :] == expert
    second = routes[1:2, :] == expert
    member = jnp.where(first, 1.0, jnp.where(second, 1.0, 0.0))
    earlier = jnp.where(iota((128, 128), 0) < iota((128, 128), 1), 1.0, 0.0).astype(BF16)
    rank = jnp.dot(member.astype(BF16), earlier, preferred_element_type=F32)
    code = (member * (rank + 1.0)).astype(BF16)
    share = jnp.where(first, weights[0:1, :], jnp.where(second, weights[1:2, :], 0.0))
    high = share.astype(BF16)
    low = (share - high.astype(F32)).astype(BF16)
    table = jnp.concatenate([code, high, low], axis=1)
    rows = PER * 8
    at = iota((rows, 128), 0)
    wanted = ((at & 3) + 1).astype(F32)
    upper = ((at >> 2) & 1) == 0
    for g in range(GROUPS):
        spread = jnp.where((at >> 3) + g * PER == iota((rows, 128), 1), 1.0, 0.0).astype(BF16)
        wide = jnp.dot(spread, table, preferred_element_type=F32)
        chosen = wide[:, :128] == wanted
        one = jnp.where(chosen, 1.0, 0.0)
        high_g = jnp.where(chosen, wide[:, 128:256], 0.0)
        low_g = jnp.where(chosen, wide[:, 256:], 0.0)
        zero = jnp.zeros_like(one)
        pack_l[g] = jnp.concatenate(
            [jnp.where(upper, one, zero), jnp.where(upper, zero, one)], axis=1
        ).astype(BF16)
        comb_l[g] = jnp.concatenate(
            [
                jnp.where(upper, high_g, zero),
                jnp.where(upper, zero, high_g),
                jnp.where(upper, low_g, zero),
                jnp.where(upper, zero, low_g),
            ],
            axis=1,
        ).astype(BF16)


def blocks(ref, lo, count):
    return ref.at[pl.ds(lo, count)]


def wait_group(buf, sem, g):
    z, y, c, x = coords()
    other = (lax.axis_index("sp"), (x + 1) % 4)

    @pl.when(g == 0)
    def _():
        part = blocks(buf, 1, PER - 1)
        pltpu.make_async_remote_copy(part, part, sem, sem, other, MESH).wait_recv()

    @pl.when(g > 0)
    def _():
        part = blocks(buf, g * PER, PER)
        pltpu.make_async_remote_copy(part, part, sem, sem, other, MESH).wait_recv()


def send_group(src, dst, send_sem, recv_sem, g, sign):
    @pl.loop(0, PER)
    def _(j):
        d = g * PER + j

        @pl.when(d > 0)
        def _():
            pltpu.make_async_remote_copy(
                src.at[d], dst.at[d], send_sem, recv_sem, peer(d, sign), MESH
            ).start()


def wait_sent(buf, sem):
    x = lax.axis_index("tp")
    part = blocks(buf, 1, GROUPS * PER - 1)
    pltpu.make_async_remote_copy(
        part, part, sem, sem, (lax.axis_index("sp"), (x + 1) % 4), MESH
    ).wait_send()


def expert_phase(stream, normed, pack_l, comb_l, gate, up, down, weight_copies, bufs, total, out):
    out_slots, in_slots, answers, replies, send_sem, recv_sem, send_back, recv_back = bufs
    halves = jnp.concatenate([normed[:, :1024], normed[:, 1024:]], axis=0)
    for g in range(GROUPS):
        with jax.named_scope("pack"):
            packed = jnp.dot(pack_l[g], halves, preferred_element_type=F32).astype(BF16)
            out_slots[pl.ds(g * PER, PER)] = packed.reshape(PER, 8, 1024)
        with jax.named_scope("dispatch"):
            send_group(out_slots, in_slots, send_sem, recv_sem.at[g], g, 1)
    in_slots[0] = out_slots[0]
    for copy in weight_copies:
        copy.wait()
    rows = PER * 8
    a, b = iota((rows, rows), 0), iota((rows, rows), 1)
    place = ((a & 127) >> 2) * 8 + (a >> 7) * 4 + (a & 3)
    unpack = jnp.where(place == b, 1.0, 0.0).astype(BF16)
    place_b = ((b & 127) >> 2) * 8 + (b >> 7) * 4 + (b & 3)
    repack = jnp.where(place_b == a, 1.0, 0.0).astype(BF16)

    @pl.loop(0, GROUPS)
    def _(g):
        with jax.named_scope("slots_wait"):
            wait_group(in_slots, recv_sem.at[g], g)
        came = in_slots[pl.ds(g * PER, PER)].reshape(rows, 1024)
        flat = jnp.dot(unpack, came, preferred_element_type=F32).astype(BF16)
        x = jnp.concatenate([flat[:128], flat[128:]], axis=1)
        hidden = []
        for n in range(0, 1024, 256):
            gated = jnp.dot(x, gate[:, n : n + 256], preferred_element_type=F32)
            lifted = jnp.dot(x, up[:, n : n + 256], preferred_element_type=F32)
            hidden.append((gated * jax.nn.sigmoid(gated) * lifted).astype(BF16))
        hidden = jnp.concatenate(hidden, axis=1)
        y0 = jnp.dot(hidden, down[:, :1024], preferred_element_type=F32).astype(BF16)
        y1 = jnp.dot(hidden, down[:, 1024:], preferred_element_type=F32).astype(BF16)
        both = jnp.concatenate([y0, y1], axis=0)
        back = jnp.dot(repack, both, preferred_element_type=F32).astype(BF16)
        answers[pl.ds(g * PER, PER)] = back.reshape(PER, 8, 1024)
        with jax.named_scope("answer_send"):
            send_group(answers, replies, send_back, recv_back.at[g], g, -1)

    replies[0] = answers[0]
    total[...] = jnp.zeros_like(total)

    @pl.loop(0, GROUPS)
    def _(g):
        with jax.named_scope("replies_wait"):
            wait_group(replies, recv_back.at[g], g)
        got = replies[pl.ds(g * PER, PER)].reshape(rows, 1024)
        total[...] += lax.dot_general(
            comb_l[g], got, (((0,), (0,)), ((), ())), preferred_element_type=F32
        )

    for h in range(2):
        part = total[h * 128 : h * 128 + 128] + total[256 + h * 128 : 256 + h * 128 + 128]
        cols = slice(h * 1024, h * 1024 + 1024)
        out[:, cols] = (stream[:, cols].astype(F32) + part).astype(BF16)
    wait_sent(out_slots, send_sem)
    wait_sent(answers, send_back)


def slot_buffers():
    slots = pltpu.VMEM((GROUPS * PER, 8, 1024), BF16)
    dma = pltpu.SemaphoreType.DMA
    return [slots] * 4 + [dma, dma((GROUPS,)), dma, dma((GROUPS,))]


def sp_peer(i):
    return (i, lax.axis_index("tp"))


def tp_peer(i):
    return (lax.axis_index("sp"), i)


def dot_nt(a, b):
    return lax.dot_general(a, b, (((1,), (1,)), ((), ())), preferred_element_type=F32)


def dot_tn(a, b):
    return lax.dot_general(a, b, (((0,), (0,)), ((), ())), preferred_element_type=F32)


def dot(a, b):
    return jnp.dot(a, b, preferred_element_type=F32)


def split(value):
    high = value.astype(BF16)
    return high, (value - high.astype(F32)).astype(BF16)


def spike_sums(spikes, run_row, run_col):
    at_or_before = jnp.where(iota((512, 512), 0) <= iota((512, 512), 1), 1.0, 0.0).astype(BF16)
    after = jnp.where(iota((512, 512), 0) >= iota((512, 512), 1), 1.0, 0.0).astype(BF16)
    rest = spikes[...]
    row, col = jnp.zeros((8, 512), F32), jnp.zeros((512, 8), F32)
    for _ in range(3):
        part = rest.astype(BF16)
        rest = rest - part.astype(F32)
        row = row + dot(part, at_or_before)
        col = col + dot_nt(after, part)
    run_row[...] = row
    run_col[...] = col


def channel_pass(query, forget, value, margin, qd, kd, vv, last):
    lower = jnp.where(iota((128, 128), 0) >= iota((128, 128), 1), 1.0, 0.0).astype(BF16)
    last[...] = jnp.zeros_like(last)

    @pl.loop(0, 4)
    def _(b):
        rows = pl.ds(pl.multiple_of(b * 128, 128), 128)
        for n in range(0, 512, 128):
            cols = slice(n, n + 128)
            keys = margin[:, cols] * jax.nn.sigmoid(-forget[rows, cols].astype(F32))
            high, low = split(jnp.log1p(-keys))
            run = dot(lower, high) + dot(lower, low) + last[:, cols]
            last[:, cols] = run[127:128]
            kd[rows, cols] = (keys * jnp.exp(-run)).astype(BF16)
            qd[rows, cols] = (query[rows, cols].astype(F32) * jnp.exp(run) * 128**-0.5).astype(BF16)
            logits = value[rows, cols].astype(F32)
            vv[rows, cols] = (logits * jax.nn.sigmoid(logits)).astype(BF16)


def own_states(kd, vv, last, run_row, run_col, state_out, decay_out):
    for h in range(4):
        cols = slice(h * 128, h * 128 + 128)
        total = run_row[h : h + 1, 511:512]
        fade = jnp.exp(total - run_col[:, h : h + 1])
        keys = (kd[:, cols].astype(F32) * fade).astype(BF16)
        state = dot_tn(vv[:, cols], keys) * jnp.exp(last[:, cols])
        state_out[pl.ds(h * 8, 8)] = state.astype(BF16).reshape(8, 16, 128)
        decay_out[h] = last[:, cols] + total


def within_pass(qd, kd, vv, run_row, run_col, local):
    causal = iota((128, 128), 0) >= iota((128, 128), 1)
    for h in range(4):
        cols = slice(h * 128, h * 128 + 128)
        for i in range(4):
            rows = slice(i * 128, i * 128 + 128)
            seen = (i + 1) * 128
            scores = dot_nt(qd[rows, cols], kd[:seen, cols])
            gap = run_col[rows, h : h + 1] - run_row[h : h + 1, :seen]
            edge = slice(i * 128, seen)
            inner = jnp.where(causal, scores[:, edge] * jnp.exp(jnp.where(causal, gap[:, edge], 0.0)), 0.0)
            parts = [inner.astype(BF16)]
            if i:
                parts.insert(0, (scores[:, : i * 128] * jnp.exp(gap[:, : i * 128])).astype(BF16))
            weights = jnp.concatenate(parts, axis=1)
            local[rows, cols] = dot(weights, vv[:seen, cols])


def send_states(state_out, decay_out, state_in, decay_in, sems):
    me = lax.axis_index("sp")
    send, recv, send_d, recv_d = sems

    @pl.loop(1, 32)
    def _(d):
        p = (me + d) % 32
        pltpu.make_async_remote_copy(
            decay_out.at[p // 8], decay_in.at[me], send_d, recv_d, sp_peer(p), MESH
        ).start()
        pltpu.make_async_remote_copy(
            state_out.at[p], state_in.at[me], send, recv, sp_peer(p), MESH
        ).start()

    state_in[me] = state_out[me]
    decay_in[me] = decay_out[me // 8]


def wait_bytes(part, sem, sent):
    copy = pltpu.make_async_remote_copy(
        part, part, sem, sem, tp_peer((lax.axis_index("tp") + 1) % 4), MESH
    )
    if sent:
        copy.wait_send()
    else:
        copy.wait_recv()


def scan_states(state_in, decay_in, prior_out, prior_in, sems, back):
    send, recv, send_d, recv_d = sems
    wait_bytes(state_in.at[pl.ds(0, 31)], recv, False)
    wait_bytes(decay_in.at[pl.ds(0, 31)], recv_d, False)
    state = jnp.zeros((16, 128), F32)
    for i in range(32):
        prior_out[i] = state.astype(BF16)
        state = jnp.exp(decay_in[i]) * state + state_in[i].astype(F32)
    me = lax.axis_index("sp")

    @pl.loop(1, 32)
    def _(d):
        p = (me + d) % 32
        pltpu.make_async_remote_copy(
            prior_out.at[p], prior_in.at[me], back[0], back[1], sp_peer(p), MESH
        ).start()

    prior_in[me] = prior_out[me]


def gate_pass(qd, run_col, local, prior_in, out_gate, head_scale, gated_out, gated_in, sems):
    x = lax.axis_index("tp")

    def block(j):
        rows = pl.ds(pl.multiple_of(j * 128, 128), 128)
        for h in range(4):
            cols = slice(h * 128, h * 128 + 128)
            asked = (qd[rows, cols].astype(F32) * jnp.exp(run_col[rows, h : h + 1])).astype(BF16)
            prior = prior_in[pl.ds(h * 8, 8)].reshape(128, 128)
            full = local[rows, cols] + dot_nt(asked, prior)
            square = jnp.mean(full * full, axis=1, keepdims=True)
            logits = out_gate[rows, cols].astype(F32)
            done = full * lax.rsqrt(square + 1e-06) * head_scale[:, cols] * (logits * jax.nn.sigmoid(logits))
            gated_out[j, :, cols] = done.astype(BF16)

    @pl.loop(0, 4)
    def _(k):
        j = (x + 2 + k) % 4
        j = jnp.where(k == 0, (x + 2) % 4, jnp.where(k == 1, (x + 1) % 4, jnp.where(k == 2, (x + 3) % 4, x)))
        block(j)

        @pl.when(k < 3)
        def _():
            pltpu.make_async_remote_copy(
                gated_out.at[j], gated_in.at[x], sems[0], sems[1].at[k], tp_peer(j), MESH
            ).start()

    gated_in[x] = gated_out[x]


def project(gated_in, matrix, mixed, sems):
    x = lax.axis_index("tp")
    mixed[...] = dot(gated_in[x], matrix[pl.ds(pl.multiple_of(x * 512, 512), 512)])
    for k, back in ((1, 3), (2, 1), (0, 2)):
        i = (x + back) % 4
        wait_bytes(gated_in.at[i], sems[1].at[k], False)
        mixed[...] += dot(gated_in[i], matrix[pl.ds(pl.multiple_of(i * 512, 512), 512)])


def layer_kernel(
    resid_hbm, query_hbm, forget_hbm, margin, spikes, value_hbm, gate_logits_hbm, head_scale,
    matrix_hbm, scale, routes, weights, gate_hbm, up_hbm, down_hbm, out,
    resid, query, forget, value, gate_logits, matrix, gate, up, down, in_sems,
    qd, kd, vv, last, run_row, run_col, local, mixed, pack_l, comb_l, total,
    state_out, state_in, prior_out, prior_in, decay_out, decay_in, gated_out, gated_in,
    state_send, state_recv, decay_send, decay_recv, prior_send, prior_recv, gated_send, gated_recv,
    *bufs,
):
    moves = [
        (forget_hbm, forget), (query_hbm, query), (value_hbm, value), (gate_logits_hbm, gate_logits),
        (resid_hbm, resid), (matrix_hbm, matrix), (gate_hbm.at[0], gate), (up_hbm.at[0], up),
        (down_hbm.at[0], down),
    ]
    copies = [pltpu.make_async_copy(src, dst, in_sems.at[i]) for i, (src, dst) in enumerate(moves)]
    for copy in copies:
        copy.start()
    with jax.named_scope("greet"):
        barrier = entry_barrier()
    with jax.named_scope("spikes"):
        spike_sums(spikes, run_row, run_col)
    with jax.named_scope("inputs"):
        for copy in copies[:3]:
            copy.wait()
    with jax.named_scope("channels"):
        channel_pass(query, forget, value, margin, qd, kd, vv, last)
    with jax.named_scope("states"):
        own_states(kd, vv, last, run_row, run_col, state_out, decay_out)
    with jax.named_scope("met"):
        pl.semaphore_wait(barrier, GROUPS * PER - 1)
    sems = (state_send, state_recv, decay_send, decay_recv)
    with jax.named_scope("state_send"):
        send_states(state_out, decay_out, state_in, decay_in, sems)
    with jax.named_scope("within"):
        within_pass(qd, kd, vv, run_row, run_col, local)
    back = (prior_send, prior_recv)
    with jax.named_scope("scan"):
        scan_states(state_in, decay_in, prior_out, prior_in, sems, back)
    with jax.named_scope("tables"):
        slot_tables(routes, weights, pack_l, comb_l)
    copies[3].wait()
    with jax.named_scope("prior_wait"):
        wait_bytes(prior_in.at[pl.ds(0, 31)], prior_recv, False)
    gated = (gated_send, gated_recv)
    with jax.named_scope("gating"):
        gate_pass(qd, run_col, local, prior_in, gate_logits, head_scale, gated_out, gated_in, gated)
    copies[4].wait()
    copies[5].wait()
    with jax.named_scope("project"):
        project(gated_in, matrix, mixed, gated)
    stream = (resid[...].astype(F32) + mixed[...]).astype(BF16)
    resid[...] = stream
    values = stream.astype(F32)
    square = jnp.mean(values * values, axis=1, keepdims=True)
    normed = (values * lax.rsqrt(square + 1e-06) * scale[...]).astype(BF16)
    with jax.named_scope("experts"):
        expert_phase(resid, normed, pack_l, comb_l, gate, up, down, copies[6:], bufs, total, out)
    wait_bytes(state_out.at[pl.ds(0, 31)], state_send, True)
    wait_bytes(decay_in.at[pl.ds(0, 31)], decay_send, True)
    wait_bytes(prior_out.at[pl.ds(0, 31)], prior_send, True)
    wait_bytes(gated_out.at[pl.ds(0, 3)], gated_send, True)


def layer(
    resid, query, forget_logits, forget_margin, decay_spike, value_logits, output_gate_logits,
    head_norm_scale, output_matrix, norm_scale_vector, routes, routing_weight, gate, up, down,
):
    vmem = pl.BlockSpec(memory_space=pltpu.VMEM)
    hbm = pl.BlockSpec(memory_space=pl.ANY)
    dma = pltpu.SemaphoreType.DMA
    wide = pltpu.VMEM((512, 512), BF16)
    pieces = pltpu.VMEM((32, 16, 128), BF16)
    return pl.pallas_call(
        layer_kernel,
        out_shape=jax.ShapeDtypeStruct((128, 2048), BF16),
        in_specs=[hbm, hbm, hbm, vmem, vmem, hbm, hbm, vmem, hbm, vmem, vmem, vmem, hbm, hbm, hbm],
        out_specs=vmem,
        scratch_shapes=[
            pltpu.VMEM((128, 2048), BF16),
            wide,
            wide,
            wide,
            wide,
            pltpu.VMEM((2048, 2048), BF16),
            pltpu.VMEM((2048, 1024), BF16),
            pltpu.VMEM((2048, 1024), BF16),
            pltpu.VMEM((1024, 2048), BF16),
            dma((9,)),
            wide,
            wide,
            wide,
            pltpu.VMEM((1, 512), F32),
            pltpu.VMEM((8, 512), F32),
            pltpu.VMEM((512, 8), F32),
            pltpu.VMEM((512, 512), F32),
            pltpu.VMEM((128, 2048), F32),
            pltpu.VMEM((GROUPS, PER * 8, 256), BF16),
            pltpu.VMEM((GROUPS, PER * 8, 512), BF16),
            pltpu.VMEM((512, 1024), F32),
            pieces,
            pieces,
            pieces,
            pieces,
            pltpu.VMEM((4, 1, 128), F32),
            pltpu.VMEM((32, 1, 128), F32),
            pltpu.VMEM((4, 128, 512), BF16),
            pltpu.VMEM((4, 128, 512), BF16),
        ]
        + [dma] * 7
        + [dma((3,))]
        + slot_buffers(),
        compiler_params=pltpu.CompilerParams(
            collective_id=0, has_side_effects=True, vmem_limit_bytes=62 * 1024 * 1024
        ),
    )(
        resid, query, forget_logits, forget_margin.reshape(1, 512),
        jnp.pad(decay_spike.T, ((0, 4), (0, 0))), value_logits, output_gate_logits,
        head_norm_scale.reshape(1, 512), output_matrix, norm_scale_vector.reshape(1, 2048),
        routes.T, routing_weight.T, gate, up, down,
    )


def solution(mesh):
    whole = ("sp", "tp")
    rows, heads, experts = P(whole, None), P("sp", "tp"), P(whole, None, None)
    return jax.shard_map(
        layer,
        mesh=mesh,
        in_specs=(
            rows, heads, heads, P("tp"), heads, heads, heads, P("tp"), P(), P(), rows, rows,
            experts, experts, experts,
        ),
        out_specs=rows,
        check_vma=False,
    )
```

time: 291 us -> 98.5 us (0.34)
  other arithmetic: 84.5 us -> 0 us
  blocking collectives: 33.5 us -> 0 us
  waiting for transfers between devices: 29.8 us -> 0 us
  matrix products: 26.7 us -> 0 us
  local copies, waits for them, and re-layouts: 22.1 us -> 3.19 us
  Pallas kernels: 78.8 us -> 95 us
  between operations: 13.6 us -> 0.01 us
    dot_general x8 -> x0, other arithmetic: 58.6 us -> none  [advance(): jnp.einsum('htk,hsk,htsk->hts', query_block, key_b, weight_t, precision=m...]
    all_gather x2 -> x0, waiting for transfers between devices: 29.8 us -> none  [carried_in(): pieces = jax.tree.map(lambda part: lax.all_gather(part, axis), so_far)]
    dot_general x26 -> x0, matrix products: 26.7 us -> none  [the longest x8 8.18 us: advance(): jnp.einsum('bup,bpl->bul', query_block * jnp.exp(cumulative_block), curre...]
    all_gather x4 -> x0, blocking collectives: 22.8 us -> none  [carried_in(): pieces = jax.tree.map(lambda part: lax.all_gather(part, axis), so_far)]
    pallas_call x1, Pallas kernels: 78.8 us -> 95 us  [layer(): pl.pallas_call(layer_kernel, out_shape=jax.ShapeDtypeStruct((128, 2048),...]
    select_n x8 -> x0, other arithmetic: 13.6 us -> none  [advance(): weight_t = jnp.where(causal, jnp.exp(jnp.where(causal, spread, 0.0)), 0.0)]
    all_to_all x1 -> x0, blocking collectives: 10.7 us -> none  [body(): lax.all_to_all(gated_rows, 'tp', split_axis=0, concat_axis=1, tiled=True)]
    dynamic_slice x32 -> x0, local copies, waits for them, and re-layouts: 9.04 us -> none  [block_recurrence(): lax.scan(advance, start_state, (queries, keys_in, values, cum_log))]
  transfers between devices with their start and end apart: 2 -> 0, of which waited for: 2 -> 0; matrix products, arithmetic and copies ran while one was open for 1% -> 0% of each run, Pallas kernels for 0% -> 0%
where the time goes in v2:
time: 98.5 us; the launch traced here: 98.2 us
  Pallas kernels  95 us (96%)
  local copies, waits for them, and re-layouts  3.19 us (3%)
    pallas_call x1, Pallas kernels, layer(): pl.pallas_call(layer_kernel, out_shape=jax.ShapeDtypeStruct((128, 2048),...  95 us

profile of v2, /device:TPU:1, one launch (start us, length us, event | category | flops | bytes accessed | tf_op | source)
XLA Modules:
  0.0 98.2 jit_solution(3811833263139011444)
XLA Ops:
  0.0 1.3 %pad.4.spikes = f32[8,512]{1,0:T(8,128)} pad(f32[4,512]{1,0:T(4,128)} %bitcast.7, f32[]{:T(128)} %constant.2.clone.1), padding=0_4x0_0 | pad | bytes 24580 | tf_op jit(solution)/shard_map/jit(_pad)/pad | solution.py:483
  1.3 95.0 %shard_map.145 = bf16[128,2048]{1,0:T(8,128)(2,1)} custom-call(bf16[128,2048]{1,0:T(8,128)(2,1)} %resid_hbm.1, bf16[512,512]{1,0:T(8,128)(2,1)} %query_hbm.1, bf16[512,512]{1,0:T(8,128)(2,1)} %forget_hbm.1, f32[1,512]{1,0:T(1,128)} %bitcast.8, f32[8,512]{1,0:T(8,128)} %pad.4.spikes, bf16[512,512]{1,0:T(8,128)(2,1)} %value_hbm.1, ...), custom_call_target="tpu_custom_call" | custom-call | tf_op jit(solution)/shard_map/pallas_call | solution.py:439
  96.3 1.9 %copy.17 = bf16[128,2048]{1,0:T(8,128)(2,1)} copy(bf16[128,2048]{1,0:T(8,128)(2,1)} %shard_map.145) | data formatting | bytes 1048576

commit v3 on v2

--- a/solution.py
+++ b/solution.py
@@ -18,23 +18,23 @@
     return sp // 8, (sp // 2) % 4, sp % 2, lax.axis_index("tp")
 
 
-def peer(d, sign):
-    z, y, c, x = coords()
-    g, j = d // PER, d % PER
-    dz, dy, dc = j // 8, (j // 2) % 4, j % 2
-    dx = (g + 8 - dz - dy) % 4
-    if sign < 0:
-        dz, dy, dx = 4 - dz, 4 - dy, 4 - dx
-    z, y, c, x = (z + dz) % 4, (y + dy) % 4, (c + dc) % 2, (x + dx) % 4
-    return ((z * 4 + y) * 2 + c, x)
+def wrap(value, size):
+    return jnp.where(value >= size, value - size, value)
 
 
 def entry_barrier():
     barrier = pltpu.get_barrier_semaphore()
-
-    @pl.loop(1, GROUPS * PER)
-    def _(d):
-        pl.semaphore_signal(barrier, inc=1, device_id=peer(d, 1), device_id_type=MESH)
+    sp, x = lax.axis_index("sp"), lax.axis_index("tp")
+    others = [wrap(x + k, 4) for k in range(1, 4)]
+    for other in others:
+        pl.semaphore_signal(barrier, inc=1, device_id=(sp, other), device_id_type=MESH)
+
+    @pl.loop(1, 32)
+    def _(p):
+        for other in [x] + others:
+            pl.semaphore_signal(
+                barrier, inc=1, device_id=(wrap(sp + p, 32), other), device_id_type=MESH
+            )
 
     return barrier
 
@@ -105,15 +105,28 @@
 
 
 def send_group(src, dst, send_sem, recv_sem, g, sign):
-    @pl.loop(0, PER)
-    def _(j):
-        d = g * PER + j
-
-        @pl.when(d > 0)
-        def _():
-            pltpu.make_async_remote_copy(
-                src.at[d], dst.at[d], send_sem, recv_sem, peer(d, sign), MESH
-            ).start()
+    z, y, c, x = coords()
+    turned = g if sign > 0 else 4 - g
+    rows = [2 * wrap(y + (dy if sign > 0 else (4 - dy) % 4), 4) for dy in range(4)]
+    cores = [c, 1 - c]
+
+    def one(dz):
+        plane = 8 * wrap(z + dz if sign > 0 else z + 4 - dz, 4)
+        start = x + turned + (4 - dz if sign > 0 else dz)
+        for dy in range(4):
+            column = (start + (4 - dy if sign > 0 else dy)) % 4
+            for dc in range(2):
+                d = g * PER + dz * 8 + dy * 2 + dc
+                copy = pltpu.make_async_remote_copy(
+                    src.at[d], dst.at[d], send_sem, recv_sem,
+                    (plane + rows[dy] + cores[dc], column), MESH,
+                )
+                if dy == 0 and dc == 0:
+                    pl.when(d > 0)(copy.start)
+                else:
+                    copy.start()
+
+    pl.loop(0, 4)(one)
 
 
 def wait_sent(buf, sem):
@@ -218,7 +231,7 @@
 def spike_sums(spikes, run_row, run_col):
     at_or_before = jnp.where(iota((512, 512), 0) <= iota((512, 512), 1), 1.0, 0.0).astype(BF16)
     after = jnp.where(iota((512, 512), 0) >= iota((512, 512), 1), 1.0, 0.0).astype(BF16)
-    rest = spikes[...]
+    rest = jnp.concatenate([spikes[...], jnp.zeros((4, 512), F32)], axis=0)
     row, col = jnp.zeros((8, 512), F32), jnp.zeros((512, 8), F32)
     for _ in range(3):
         part = rest.astype(BF16)
@@ -283,7 +296,7 @@
 
     @pl.loop(1, 32)
     def _(d):
-        p = (me + d) % 32
+        p = wrap(me + d, 32)
         pltpu.make_async_remote_copy(
             decay_out.at[p // 8], decay_in.at[me], send_d, recv_d, sp_peer(p), MESH
         ).start()
@@ -317,7 +330,7 @@
 
     @pl.loop(1, 32)
     def _(d):
-        p = (me + d) % 32
+        p = wrap(me + d, 32)
         pltpu.make_async_remote_copy(
             prior_out.at[p], prior_in.at[me], back[0], back[1], sp_peer(p), MESH
         ).start()
@@ -325,41 +338,43 @@
     prior_in[me] = prior_out[me]
 
 
-def gate_pass(qd, run_col, local, prior_in, out_gate, head_scale, gated_out, gated_in, sems):
+def gate_factors(qd, run_col, out_gate, head_scale, factor):
+    @pl.loop(0, 4)
+    def _(b):
+        rows = pl.ds(pl.multiple_of(b * 128, 128), 128)
+        for h in range(4):
+            cols = slice(h * 128, h * 128 + 128)
+            logits = out_gate[rows, cols].astype(F32)
+            factor[rows, cols] = head_scale[:, cols] * (logits * jax.nn.sigmoid(logits))
+            qd[rows, cols] = (
+                qd[rows, cols].astype(F32) * jnp.exp(run_col[rows, h : h + 1])
+            ).astype(BF16)
+
+
+def gate_pass(asked, local, prior_in, factor, gated_out, gated_in, sems):
     x = lax.axis_index("tp")
-
-    def block(j):
+    for k, ahead in enumerate((2, 1, 3, 0)):
+        j = wrap(x + ahead, 4)
         rows = pl.ds(pl.multiple_of(j * 128, 128), 128)
         for h in range(4):
             cols = slice(h * 128, h * 128 + 128)
-            asked = (qd[rows, cols].astype(F32) * jnp.exp(run_col[rows, h : h + 1])).astype(BF16)
             prior = prior_in[pl.ds(h * 8, 8)].reshape(128, 128)
-            full = local[rows, cols] + dot_nt(asked, prior)
+            full = local[rows, cols] + dot_nt(asked[rows, cols], prior)
             square = jnp.mean(full * full, axis=1, keepdims=True)
-            logits = out_gate[rows, cols].astype(F32)
-            done = full * lax.rsqrt(square + 1e-06) * head_scale[:, cols] * (logits * jax.nn.sigmoid(logits))
-            gated_out[j, :, cols] = done.astype(BF16)
-
-    @pl.loop(0, 4)
-    def _(k):
-        j = (x + 2 + k) % 4
-        j = jnp.where(k == 0, (x + 2) % 4, jnp.where(k == 1, (x + 1) % 4, jnp.where(k == 2, (x + 3) % 4, x)))
-        block(j)
-
-        @pl.when(k < 3)
-        def _():
+            gated_out[j, :, cols] = (full * lax.rsqrt(square + 1e-06) * factor[rows, cols]).astype(BF16)
+        if ahead:
             pltpu.make_async_remote_copy(
                 gated_out.at[j], gated_in.at[x], sems[0], sems[1].at[k], tp_peer(j), MESH
             ).start()
-
-    gated_in[x] = gated_out[x]
+        else:
+            gated_in[x] = gated_out[x]
 
 
 def project(gated_in, matrix, mixed, sems):
     x = lax.axis_index("tp")
     mixed[...] = dot(gated_in[x], matrix[pl.ds(pl.multiple_of(x * 512, 512), 512)])
     for k, back in ((1, 3), (2, 1), (0, 2)):
-        i = (x + back) % 4
+        i = wrap(x + back, 4)
         wait_bytes(gated_in.at[i], sems[1].at[k], False)
         mixed[...] += dot(gated_in[i], matrix[pl.ds(pl.multiple_of(i * 512, 512), 512)])
 
@@ -368,7 +383,7 @@
     resid_hbm, query_hbm, forget_hbm, margin, spikes, value_hbm, gate_logits_hbm, head_scale,
     matrix_hbm, scale, routes, weights, gate_hbm, up_hbm, down_hbm, out,
     resid, query, forget, value, gate_logits, matrix, gate, up, down, in_sems,
-    qd, kd, vv, last, run_row, run_col, local, mixed, pack_l, comb_l, total,
+    qd, kd, vv, last, run_row, run_col, local, factor, mixed, pack_l, comb_l, total,
     state_out, state_in, prior_out, prior_in, decay_out, decay_in, gated_out, gated_in,
     state_send, state_recv, decay_send, decay_recv, prior_send, prior_recv, gated_send, gated_recv,
     *bufs,
@@ -399,17 +414,19 @@
         send_states(state_out, decay_out, state_in, decay_in, sems)
     with jax.named_scope("within"):
         within_pass(qd, kd, vv, run_row, run_col, local)
+    with jax.named_scope("tables"):
+        slot_tables(routes, weights, pack_l, comb_l)
+    with jax.named_scope("factors"):
+        copies[3].wait()
+        gate_factors(qd, run_col, gate_logits, head_scale, factor)
     back = (prior_send, prior_recv)
     with jax.named_scope("scan"):
         scan_states(state_in, decay_in, prior_out, prior_in, sems, back)
-    with jax.named_scope("tables"):
-        slot_tables(routes, weights, pack_l, comb_l)
-    copies[3].wait()
     with jax.named_scope("prior_wait"):
         wait_bytes(prior_in.at[pl.ds(0, 31)], prior_recv, False)
     gated = (gated_send, gated_recv)
     with jax.named_scope("gating"):
-        gate_pass(qd, run_col, local, prior_in, gate_logits, head_scale, gated_out, gated_in, gated)
+        gate_pass(qd, local, prior_in, factor, gated_out, gated_in, gated)
     copies[4].wait()
     copies[5].wait()
     with jax.named_scope("project"):
@@ -438,7 +455,7 @@
     pieces = pltpu.VMEM((32, 16, 128), BF16)
     return pl.pallas_call(
         layer_kernel,
-        out_shape=jax.ShapeDtypeStruct((128, 2048), BF16),
+        out_shape=pltpu.VMEM((128, 2048), BF16),
         in_specs=[hbm, hbm, hbm, vmem, vmem, hbm, hbm, vmem, hbm, vmem, vmem, vmem, hbm, hbm, hbm],
         out_specs=vmem,
         scratch_shapes=[
@@ -458,6 +475,7 @@
             pltpu.VMEM((1, 512), F32),
             pltpu.VMEM((8, 512), F32),
             pltpu.VMEM((512, 8), F32),
+            pltpu.VMEM((512, 512), F32),
             pltpu.VMEM((512, 512), F32),
             pltpu.VMEM((128, 2048), F32),
             pltpu.VMEM((GROUPS, PER * 8, 256), BF16),
@@ -480,7 +498,7 @@
         ),
     )(
         resid, query, forget_logits, forget_margin.reshape(1, 512),
-        jnp.pad(decay_spike.T, ((0, 4), (0, 0))), value_logits, output_gate_logits,
+        decay_spike.T, value_logits, output_gate_logits,
         head_norm_scale.reshape(1, 512), output_matrix, norm_scale_vector.reshape(1, 2048),
         routes.T, routing_weight.T, gate, up, down,
     )

time: 98.5 us -> 82.7 us (0.84)
  Pallas kernels: 95 us -> 81.7 us
  local copies, waits for them, and re-layouts: 3.19 us -> 0.8 us
    pallas_call x1, Pallas kernels: 95 us -> 81.7 us  [layer(): pl.pallas_call(layer_kernel, out_shape=pltpu.VMEM((128, 2048), BF16), in_...]
    pad x1 -> x0, local copies, waits for them, and re-layouts: 1.31 us -> none  [layer(): jnp.pad(decay_spike.T, ((0, 4), (0, 0)))]
    unnamed x1, local copies, waits for them, and re-layouts: 1.88 us -> 0.8 us
where the time goes in v3:
time: 82.7 us; the launch traced here: 82.5 us
  Pallas kernels  81.7 us (99%)
    pallas_call x1, Pallas kernels, layer(): pl.pallas_call(layer_kernel, out_shape=pltpu.VMEM((128, 2048), BF16), in_...  81.7 us

profile of v3, /device:TPU:1, one launch (start us, length us, event | category | flops | bytes accessed | tf_op | source)
XLA Modules:
  0.0 82.5 jit_solution(14557963115299728670)
XLA Ops:
  0.0 81.7 %shard_map.145 = bf16[128,2048]{1,0:T(8,128)(2,1)S(1)} custom-call(bf16[128,2048]{1,0:T(8,128)(2,1)} %resid_hbm.1, bf16[512,512]{1,0:T(8,128)(2,1)} %query_hbm.1, bf16[512,512]{1,0:T(8,128)(2,1)} %forget_hbm.1, f32[1,512]{1,0:T(1,128)} %bitcast.8, f32[4,512]{1,0:T(4,128)} %bitcast.6, bf16[512,512]{1,0:T(8,128)(2,1)} %value_hbm.1, ...), custom_call_target="tpu_custom_call" | custom-call | tf_op jit(solution)/shard_map/pallas_call | solution.py:456
  81.7 0.8 copy.17

commit v4 on v3

--- a/solution.py
+++ b/solution.py
@@ -25,17 +25,15 @@
 def entry_barrier():
     barrier = pltpu.get_barrier_semaphore()
     sp, x = lax.axis_index("sp"), lax.axis_index("tp")
-    others = [wrap(x + k, 4) for k in range(1, 4)]
-    for other in others:
-        pl.semaphore_signal(barrier, inc=1, device_id=(sp, other), device_id_type=MESH)
-
-    @pl.loop(1, 32)
-    def _(p):
-        for other in [x] + others:
-            pl.semaphore_signal(
-                barrier, inc=1, device_id=(wrap(sp + p, 32), other), device_id_type=MESH
-            )
-
+
+    for low, top in ((16, 32), (1, 16)):
+
+        @pl.loop(low, top)
+        def _(p):
+            pl.semaphore_signal(barrier, inc=1, device_id=(wrap(sp + p, 32), x), device_id_type=MESH)
+
+    for k in range(1, 4):
+        pl.semaphore_signal(barrier, inc=1, device_id=(sp, wrap(x + k, 4)), device_id_type=MESH)
     return barrier
 
 
@@ -56,9 +54,7 @@
     rank = jnp.dot(member.astype(BF16), earlier, preferred_element_type=F32)
     code = (member * (rank + 1.0)).astype(BF16)
     share = jnp.where(first, weights[0:1, :], jnp.where(second, weights[1:2, :], 0.0))
-    high = share.astype(BF16)
-    low = (share - high.astype(F32)).astype(BF16)
-    table = jnp.concatenate([code, high, low], axis=1)
+    table = jnp.concatenate([code, share.astype(BF16)], axis=1)
     rows = PER * 8
     at = iota((rows, 128), 0)
     wanted = ((at & 3) + 1).astype(F32)
@@ -68,20 +64,13 @@
         wide = jnp.dot(spread, table, preferred_element_type=F32)
         chosen = wide[:, :128] == wanted
         one = jnp.where(chosen, 1.0, 0.0)
-        high_g = jnp.where(chosen, wide[:, 128:256], 0.0)
-        low_g = jnp.where(chosen, wide[:, 256:], 0.0)
+        weighed = jnp.where(chosen, wide[:, 128:], 0.0)
         zero = jnp.zeros_like(one)
         pack_l[g] = jnp.concatenate(
             [jnp.where(upper, one, zero), jnp.where(upper, zero, one)], axis=1
         ).astype(BF16)
         comb_l[g] = jnp.concatenate(
-            [
-                jnp.where(upper, high_g, zero),
-                jnp.where(upper, zero, high_g),
-                jnp.where(upper, low_g, zero),
-                jnp.where(upper, zero, low_g),
-            ],
-            axis=1,
+            [jnp.where(upper, weighed, zero), jnp.where(upper, zero, weighed)], axis=1
         ).astype(BF16)
 
 
@@ -167,7 +156,7 @@
         for n in range(0, 1024, 256):
             gated = jnp.dot(x, gate[:, n : n + 256], preferred_element_type=F32)
             lifted = jnp.dot(x, up[:, n : n + 256], preferred_element_type=F32)
-            hidden.append((gated * jax.nn.sigmoid(gated) * lifted).astype(BF16))
+            hidden.append((gated * logistic(gated) * lifted).astype(BF16))
         hidden = jnp.concatenate(hidden, axis=1)
         y0 = jnp.dot(hidden, down[:, :1024], preferred_element_type=F32).astype(BF16)
         y1 = jnp.dot(hidden, down[:, 1024:], preferred_element_type=F32).astype(BF16)
@@ -180,19 +169,19 @@
     replies[0] = answers[0]
     total[...] = jnp.zeros_like(total)
 
-    @pl.loop(0, GROUPS)
-    def _(g):
+    def gathered(g):
         with jax.named_scope("replies_wait"):
             wait_group(replies, recv_back.at[g], g)
-        got = replies[pl.ds(g * PER, PER)].reshape(rows, 1024)
-        total[...] += lax.dot_general(
-            comb_l[g], got, (((0,), (0,)), ((), ())), preferred_element_type=F32
-        )
-
+        return dot_tn(comb_l[g], replies[pl.ds(g * PER, PER)].reshape(rows, 1024))
+
+    @pl.loop(0, GROUPS - 1)
+    def _(g):
+        total[...] += gathered(g)
+
+    summed = total[...] + gathered(GROUPS - 1)
     for h in range(2):
-        part = total[h * 128 : h * 128 + 128] + total[256 + h * 128 : 256 + h * 128 + 128]
         cols = slice(h * 1024, h * 1024 + 1024)
-        out[:, cols] = (stream[:, cols].astype(F32) + part).astype(BF16)
+        out[:, cols] = (stream[:, cols].astype(F32) + summed[h * 128 : h * 128 + 128]).astype(BF16)
     wait_sent(out_slots, send_sem)
     wait_sent(answers, send_back)
 
@@ -228,48 +217,51 @@
     return high, (value - high.astype(F32)).astype(BF16)
 
 
-def spike_sums(spikes, run_row, run_col):
-    at_or_before = jnp.where(iota((512, 512), 0) <= iota((512, 512), 1), 1.0, 0.0).astype(BF16)
-    after = jnp.where(iota((512, 512), 0) >= iota((512, 512), 1), 1.0, 0.0).astype(BF16)
-    rest = jnp.concatenate([spikes[...], jnp.zeros((4, 512), F32)], axis=0)
-    row, col = jnp.zeros((8, 512), F32), jnp.zeros((512, 8), F32)
-    for _ in range(3):
-        part = rest.astype(BF16)
-        rest = rest - part.astype(F32)
-        row = row + dot(part, at_or_before)
-        col = col + dot_nt(after, part)
+def logistic(value):
+    return 0.5 * jnp.tanh(0.5 * value) + 0.5
+
+
+def fill_triangle(tri):
+    tri[...] = jnp.where(iota((256, 256), 0) >= iota((256, 256), 1), 1.0, 0.0).astype(BF16)
+
+
+def spike_sums(spikes, tri, run_row, run_col):
+    high, low = split(jnp.concatenate([spikes[...], jnp.zeros((4, 512), F32)], axis=0))
+    parts = jnp.concatenate([high[:, :256], low[:, :256], high[:, 256:], low[:, 256:]], axis=0)
+    sums = dot_nt(parts, tri[...])
+    early = sums[:8] + sums[8:16]
+    row = jnp.concatenate([early, sums[16:24] + sums[24:] + early[:, 255:256]], axis=1)
     run_row[...] = row
-    run_col[...] = col
-
-
-def channel_pass(query, forget, value, margin, qd, kd, vv, last):
-    lower = jnp.where(iota((128, 128), 0) >= iota((128, 128), 1), 1.0, 0.0).astype(BF16)
-    last[...] = jnp.zeros_like(last)
-
-    @pl.loop(0, 4)
-    def _(b):
-        rows = pl.ds(pl.multiple_of(b * 128, 128), 128)
-        for n in range(0, 512, 128):
-            cols = slice(n, n + 128)
-            keys = margin[:, cols] * jax.nn.sigmoid(-forget[rows, cols].astype(F32))
-            high, low = split(jnp.log1p(-keys))
-            run = dot(lower, high) + dot(lower, low) + last[:, cols]
-            last[:, cols] = run[127:128]
-            kd[rows, cols] = (keys * jnp.exp(-run)).astype(BF16)
-            qd[rows, cols] = (query[rows, cols].astype(F32) * jnp.exp(run) * 128**-0.5).astype(BF16)
-            logits = value[rows, cols].astype(F32)
-            vv[rows, cols] = (logits * jax.nn.sigmoid(logits)).astype(BF16)
-
-
-def own_states(kd, vv, last, run_row, run_col, state_out, decay_out):
+    run_col[...] = row.T
+
+
+def key_head(h, forget, value, margin, tri, run_row, fade, runs, kd, vv, state_out, decay_out):
+    cols = slice(h * 128, h * 128 + 128)
+    keys = margin[:, cols] * logistic(-forget[:, cols].astype(F32))
+    logs = jnp.concatenate(split(jnp.log1p(-keys)), axis=1)
+    early, late = dot(tri[...], logs[:256]), dot(tri[...], logs[256:])
+    early = early[:, :128] + early[:, 128:]
+    run = jnp.concatenate([early, late[:, :128] + late[:, 128:] + early[255:]], axis=0)
+    runs[:, cols] = run
+    raised = keys * jnp.exp(-run)
+    kd[:, cols] = raised.astype(BF16)
+    logits = value[:, cols].astype(F32)
+    values = (logits * logistic(logits)).astype(BF16)
+    vv[:, cols] = values
+    last = run[511:512]
+    state = dot_tn(values, (raised * fade[:, h : h + 1]).astype(BF16)) * jnp.exp(last)
+    state_out[pl.ds(h * 8, 8)] = state.astype(BF16).reshape(8, 16, 128)
+    decay_out[h] = last + run_row[h : h + 1, 511:512]
+
+
+def query_pass(query, runs, run_col, qd, asked):
+    grow = jnp.exp(run_col[...])
     for h in range(4):
         cols = slice(h * 128, h * 128 + 128)
-        total = run_row[h : h + 1, 511:512]
-        fade = jnp.exp(total - run_col[:, h : h + 1])
-        keys = (kd[:, cols].astype(F32) * fade).astype(BF16)
-        state = dot_tn(vv[:, cols], keys) * jnp.exp(last[:, cols])
-        state_out[pl.ds(h * 8, 8)] = state.astype(BF16).reshape(8, 16, 128)
-        decay_out[h] = last[:, cols] + total
+        faded = query[:, cols].astype(F32) * (jnp.exp(runs[:, cols]) * 128**-0.5)
+        twice = slice(h * 256, h * 256 + 256)
+        qd[:, twice] = jnp.concatenate(split(faded), axis=1)
+        asked[:, twice] = jnp.concatenate(split(faded * grow[:, h : h + 1]), axis=1)
 
 
 def within_pass(qd, kd, vv, run_row, run_col, local):
@@ -279,7 +271,10 @@
         for i in range(4):
             rows = slice(i * 128, i * 128 + 128)
             seen = (i + 1) * 128
-            scores = dot_nt(qd[rows, cols], kd[:seen, cols])
+            keys = kd[:seen, cols]
+            scores = dot_nt(
+                qd[rows, h * 256 : h * 256 + 256], jnp.concatenate([keys, keys], axis=1)
+            )
             gap = run_col[rows, h : h + 1] - run_row[h : h + 1, :seen]
             edge = slice(i * 128, seen)
             inner = jnp.where(causal, scores[:, edge] * jnp.exp(jnp.where(causal, gap[:, edge], 0.0)), 0.0)
@@ -293,16 +288,17 @@
 def send_states(state_out, decay_out, state_in, decay_in, sems):
     me = lax.axis_index("sp")
     send, recv, send_d, recv_d = sems
-
-    @pl.loop(1, 32)
-    def _(d):
-        p = wrap(me + d, 32)
-        pltpu.make_async_remote_copy(
-            decay_out.at[p // 8], decay_in.at[me], send_d, recv_d, sp_peer(p), MESH
-        ).start()
-        pltpu.make_async_remote_copy(
-            state_out.at[p], state_in.at[me], send, recv, sp_peer(p), MESH
-        ).start()
+    for low, top in ((16, 32), (1, 16)):
+
+        @pl.loop(low, top)
+        def _(d):
+            p = wrap(me + d, 32)
+            pltpu.make_async_remote_copy(
+                state_out.at[p], state_in.at[me], send, recv, sp_peer(p), MESH
+            ).start()
+            pltpu.make_async_remote_copy(
+                decay_out.at[p // 8], decay_in.at[me], send_d, recv_d, sp_peer(p), MESH
+            ).start()
 
     state_in[me] = state_out[me]
     decay_in[me] = decay_out[me // 8]
@@ -328,27 +324,21 @@
         state = jnp.exp(decay_in[i]) * state + state_in[i].astype(F32)
     me = lax.axis_index("sp")
 
-    @pl.loop(1, 32)
-    def _(d):
-        p = wrap(me + d, 32)
-        pltpu.make_async_remote_copy(
-            prior_out.at[p], prior_in.at[me], back[0], back[1], sp_peer(p), MESH
-        ).start()
+    for low, top in ((16, 32), (1, 16)):
+
+        @pl.loop(low, top)
+        def _(d):
+            p = wrap(me + d, 32)
+            pltpu.make_async_remote_copy(
+                prior_out.at[p], prior_in.at[me], back[0], back[1], sp_peer(p), MESH
+            ).start()
 
     prior_in[me] = prior_out[me]
 
 
-def gate_factors(qd, run_col, out_gate, head_scale, factor):
-    @pl.loop(0, 4)
-    def _(b):
-        rows = pl.ds(pl.multiple_of(b * 128, 128), 128)
-        for h in range(4):
-            cols = slice(h * 128, h * 128 + 128)
-            logits = out_gate[rows, cols].astype(F32)
-            factor[rows, cols] = head_scale[:, cols] * (logits * jax.nn.sigmoid(logits))
-            qd[rows, cols] = (
-                qd[rows, cols].astype(F32) * jnp.exp(run_col[rows, h : h + 1])
-            ).astype(BF16)
+def gate_factors(out_gate, head_scale, factor):
+    logits = out_gate[...].astype(F32)
+    factor[...] = head_scale[...] * (logits * logistic(logits))
 
 
 def gate_pass(asked, local, prior_in, factor, gated_out, gated_in, sems):
@@ -359,7 +349,8 @@
         for h in range(4):
             cols = slice(h * 128, h * 128 + 128)
             prior = prior_in[pl.ds(h * 8, 8)].reshape(128, 128)
-            full = local[rows, cols] + dot_nt(asked[rows, cols], prior)
+            ask = asked[rows, h * 256 : h * 256 + 256]
+            full = local[rows, cols] + dot_nt(ask, jnp.concatenate([prior, prior], axis=1))
             square = jnp.mean(full * full, axis=1, keepdims=True)
             gated_out[j, :, cols] = (full * lax.rsqrt(square + 1e-06) * factor[rows, cols]).astype(BF16)
         if ahead:
@@ -372,63 +363,81 @@
 
 def project(gated_in, matrix, mixed, sems):
     x = lax.axis_index("tp")
-    mixed[...] = dot(gated_in[x], matrix[pl.ds(pl.multiple_of(x * 512, 512), 512)])
-    for k, back in ((1, 3), (2, 1), (0, 2)):
+
+    def product(i):
+        return dot(gated_in[i], matrix[pl.ds(pl.multiple_of(i * 512, 512), 512)])
+
+    mixed[...] = product(x)
+    for k, back in ((0, 2), (1, 3), (2, 1)):
         i = wrap(x + back, 4)
-        wait_bytes(gated_in.at[i], sems[1].at[k], False)
-        mixed[...] += dot(gated_in[i], matrix[pl.ds(pl.multiple_of(i * 512, 512), 512)])
+        with jax.named_scope(f"tp_wait{k}"):
+            wait_bytes(gated_in.at[i], sems[1].at[k], False)
+        mixed[...] += product(i)
 
 
 def layer_kernel(
-    resid_hbm, query_hbm, forget_hbm, margin, spikes, value_hbm, gate_logits_hbm, head_scale,
-    matrix_hbm, scale, routes, weights, gate_hbm, up_hbm, down_hbm, out,
-    resid, query, forget, value, gate_logits, matrix, gate, up, down, in_sems,
-    qd, kd, vv, last, run_row, run_col, local, factor, mixed, pack_l, comb_l, total,
+    resid_hbm, query_hbm, forget_hbm, margin_hbm, spikes_hbm, value_hbm, gate_logits_hbm, head_scale_hbm,
+    matrix_hbm, scale_hbm, routes_hbm, weights_hbm, gate_hbm, up_hbm, down_hbm, out,
+    resid, query, forget, margin, spikes, value, gate_logits, head_scale, matrix, scale, routes,
+    weights, gate, up, down, in_sems,
+    tri, runs, qd, asked, kd, vv, run_row, run_col, local, factor, mixed, pack_l, comb_l, total,
     state_out, state_in, prior_out, prior_in, decay_out, decay_in, gated_out, gated_in,
     state_send, state_recv, decay_send, decay_recv, prior_send, prior_recv, gated_send, gated_recv,
     *bufs,
 ):
     moves = [
-        (forget_hbm, forget), (query_hbm, query), (value_hbm, value), (gate_logits_hbm, gate_logits),
-        (resid_hbm, resid), (matrix_hbm, matrix), (gate_hbm.at[0], gate), (up_hbm.at[0], up),
-        (down_hbm.at[0], down),
+        (spikes_hbm, spikes), (margin_hbm, margin), (forget_hbm, forget), (value_hbm, value),
+        (query_hbm, query), (routes_hbm, routes), (weights_hbm, weights), (gate_logits_hbm, gate_logits),
+        (head_scale_hbm, head_scale), (resid_hbm, resid), (scale_hbm, scale), (matrix_hbm, matrix),
+        (gate_hbm.at[0], gate), (up_hbm.at[0], up), (down_hbm.at[0], down),
     ]
     copies = [pltpu.make_async_copy(src, dst, in_sems.at[i]) for i, (src, dst) in enumerate(moves)]
-    for copy in copies:
+    for copy in copies[:5]:
         copy.start()
     with jax.named_scope("greet"):
         barrier = entry_barrier()
+    for copy in copies[5:]:
+        copy.start()
+    with jax.named_scope("triangle"):
+        fill_triangle(tri)
+    copies[0].wait()
     with jax.named_scope("spikes"):
-        spike_sums(spikes, run_row, run_col)
+        spike_sums(spikes, tri, run_row, run_col)
+        fade = jnp.exp(run_col[511:512, :] - run_col[...])
     with jax.named_scope("inputs"):
-        for copy in copies[:3]:
+        for copy in copies[1:4]:
             copy.wait()
-    with jax.named_scope("channels"):
-        channel_pass(query, forget, value, margin, qd, kd, vv, last)
-    with jax.named_scope("states"):
-        own_states(kd, vv, last, run_row, run_col, state_out, decay_out)
+    with jax.named_scope("keys"):
+        for h in range(4):
+            key_head(h, forget, value, margin, tri, run_row, fade, runs, kd, vv, state_out, decay_out)
     with jax.named_scope("met"):
-        pl.semaphore_wait(barrier, GROUPS * PER - 1)
+        pl.semaphore_wait(barrier, 34)
     sems = (state_send, state_recv, decay_send, decay_recv)
     with jax.named_scope("state_send"):
         send_states(state_out, decay_out, state_in, decay_in, sems)
+    with jax.named_scope("query"):
+        copies[4].wait()
+        query_pass(query, runs, run_col, qd, asked)
     with jax.named_scope("within"):
         within_pass(qd, kd, vv, run_row, run_col, local)
-    with jax.named_scope("tables"):
-        slot_tables(routes, weights, pack_l, comb_l)
-    with jax.named_scope("factors"):
-        copies[3].wait()
-        gate_factors(qd, run_col, gate_logits, head_scale, factor)
     back = (prior_send, prior_recv)
     with jax.named_scope("scan"):
         scan_states(state_in, decay_in, prior_out, prior_in, sems, back)
+    with jax.named_scope("tables"):
+        copies[5].wait()
+        copies[6].wait()
+        slot_tables(routes, weights, pack_l, comb_l)
+    with jax.named_scope("factors"):
+        copies[7].wait()
+        copies[8].wait()
+        gate_factors(gate_logits, head_scale, factor)
     with jax.named_scope("prior_wait"):
         wait_bytes(prior_in.at[pl.ds(0, 31)], prior_recv, False)
     gated = (gated_send, gated_recv)
     with jax.named_scope("gating"):
-        gate_pass(qd, local, prior_in, factor, gated_out, gated_in, gated)
-    copies[4].wait()
-    copies[5].wait()
+        gate_pass(asked, local, prior_in, factor, gated_out, gated_in, gated)
+    for copy in copies[9:12]:
+        copy.wait()
     with jax.named_scope("project"):
         project(gated_in, matrix, mixed, gated)
     stream = (resid[...].astype(F32) + mixed[...]).astype(BF16)
@@ -437,7 +446,7 @@
     square = jnp.mean(values * values, axis=1, keepdims=True)
     normed = (values * lax.rsqrt(square + 1e-06) * scale[...]).astype(BF16)
     with jax.named_scope("experts"):
-        expert_phase(resid, normed, pack_l, comb_l, gate, up, down, copies[6:], bufs, total, out)
+        expert_phase(resid, normed, pack_l, comb_l, gate, up, down, copies[12:], bufs, total, out)
     wait_bytes(state_out.at[pl.ds(0, 31)], state_send, True)
     wait_bytes(decay_in.at[pl.ds(0, 31)], decay_send, True)
     wait_bytes(prior_out.at[pl.ds(0, 31)], prior_send, True)
@@ -456,31 +465,39 @@
     return pl.pallas_call(
         layer_kernel,
         out_shape=pltpu.VMEM((128, 2048), BF16),
-        in_specs=[hbm, hbm, hbm, vmem, vmem, hbm, hbm, vmem, hbm, vmem, vmem, vmem, hbm, hbm, hbm],
+        in_specs=[hbm] * 15,
         out_specs=vmem,
         scratch_shapes=[
             pltpu.VMEM((128, 2048), BF16),
             wide,
             wide,
+            pltpu.VMEM((1, 512), F32),
+            pltpu.VMEM((4, 512), F32),
             wide,
             wide,
+            pltpu.VMEM((1, 512), F32),
             pltpu.VMEM((2048, 2048), BF16),
+            pltpu.VMEM((1, 2048), F32),
+            pltpu.VMEM((2, 128), I32),
+            pltpu.VMEM((2, 128), F32),
             pltpu.VMEM((2048, 1024), BF16),
             pltpu.VMEM((2048, 1024), BF16),
             pltpu.VMEM((1024, 2048), BF16),
-            dma((9,)),
+            dma((15,)),
+            pltpu.VMEM((256, 256), BF16),
+            pltpu.VMEM((512, 512), F32),
+            pltpu.VMEM((512, 1024), BF16),
+            pltpu.VMEM((512, 1024), BF16),
             wide,
             wide,
-            wide,
-            pltpu.VMEM((1, 512), F32),
             pltpu.VMEM((8, 512), F32),
             pltpu.VMEM((512, 8), F32),
             pltpu.VMEM((512, 512), F32),
             pltpu.VMEM((512, 512), F32),
             pltpu.VMEM((128, 2048), F32),
             pltpu.VMEM((GROUPS, PER * 8, 256), BF16),
-            pltpu.VMEM((GROUPS, PER * 8, 512), BF16),
-            pltpu.VMEM((512, 1024), F32),
+            pltpu.VMEM((GROUPS, PER * 8, 256), BF16),
+            pltpu.VMEM((256, 1024), F32),
             pieces,
             pieces,
             pieces,

time: 82.7 us -> 79.8 us (0.965)
  Pallas kernels: 81.7 us -> 78.9 us
    pallas_call x1, Pallas kernels: 81.7 us -> 78.9 us  [layer(): pl.pallas_call(layer_kernel, out_shape=pltpu.VMEM((128, 2048), BF16), in_...]
where the time goes in v4:
time: 79.8 us; the launch traced here: 79.7 us
  Pallas kernels  78.9 us (99%)
  local copies, waits for them, and re-layouts  0.8 us (1%)
    pallas_call x1, Pallas kernels, layer(): pl.pallas_call(layer_kernel, out_shape=pltpu.VMEM((128, 2048), BF16), in_...  78.9 us

profile of v4, /device:TPU:1, one launch (start us, length us, event | category | flops | bytes accessed | tf_op | source)
XLA Modules:
  0.0 79.7 jit_solution(8691234573494499179)
XLA Ops:
  0.0 78.9 %shard_map.145 = bf16[128,2048]{1,0:T(8,128)(2,1)S(1)} custom-call(bf16[128,2048]{1,0:T(8,128)(2,1)} %resid_hbm.1, bf16[512,512]{1,0:T(8,128)(2,1)} %query_hbm.1, bf16[512,512]{1,0:T(8,128)(2,1)} %forget_hbm.1, f32[1,512]{1,0:T(1,128)} %bitcast.8, f32[4,512]{1,0:T(4,128)} %bitcast.6, bf16[512,512]{1,0:T(8,128)(2,1)} %value_hbm.1, ...), custom_call_target="tpu_custom_call" | custom-call | tf_op jit(solution)/shard_map/pallas_call | solution.py:465
  78.9 0.8 copy.17

commit v5 on v4

--- a/solution.py
+++ b/solution.py
@@ -102,7 +102,7 @@
     def one(dz):
         plane = 8 * wrap(z + dz if sign > 0 else z + 4 - dz, 4)
         start = x + turned + (4 - dz if sign > 0 else dz)
-        for dy in range(4):
+        for dy in (2, 1, 3, 0):
             column = (start + (4 - dy if sign > 0 else dy)) % 4
             for dc in range(2):
                 d = g * PER + dz * 8 + dy * 2 + dc
@@ -115,7 +115,7 @@
                 else:
                     copy.start()
 
-    pl.loop(0, 4)(one)
+    pl.loop(0, 4)(lambda k: one(wrap(k + 2, 4)))
 
 
 def wait_sent(buf, sem):
@@ -361,18 +361,21 @@
             gated_in[x] = gated_out[x]
 
 
-def project(gated_in, matrix, mixed, sems):
+def project(gated_in, matrix, resid, mixed, sems):
     x = lax.axis_index("tp")
 
     def product(i):
         return dot(gated_in[i], matrix[pl.ds(pl.multiple_of(i * 512, 512), 512)])
 
-    mixed[...] = product(x)
-    for k, back in ((0, 2), (1, 3), (2, 1)):
+    mixed[...] = resid[...].astype(F32) + product(x)
+    def arrived(k, back):
         i = wrap(x + back, 4)
-        with jax.named_scope(f"tp_wait{k}"):
-            wait_bytes(gated_in.at[i], sems[1].at[k], False)
-        mixed[...] += product(i)
+        wait_bytes(gated_in.at[i], sems[1].at[k], False)
+        return product(i)
+
+    mixed[...] += arrived(0, 2)
+    mixed[...] += arrived(1, 3)
+    return (mixed[...] + arrived(2, 1)).astype(BF16)
 
 
 def layer_kernel(
@@ -439,8 +442,7 @@
     for copy in copies[9:12]:
         copy.wait()
     with jax.named_scope("project"):
-        project(gated_in, matrix, mixed, gated)
-    stream = (resid[...].astype(F32) + mixed[...]).astype(BF16)
+        stream = project(gated_in, matrix, resid, mixed, gated)
     resid[...] = stream
     values = stream.astype(F32)
     square = jnp.mean(values * values, axis=1, keepdims=True)

time: 79.8 us -> 79.6 us (level)
  no operation moved by 1% of the time
where the time goes in v5:
time: 79.6 us; the launch traced here: 79.5 us
  Pallas kernels  78.7 us (99%)
  local copies, waits for them, and re-layouts  0.8 us (1%)
    pallas_call x1, Pallas kernels, layer(): pl.pallas_call(layer_kernel, out_shape=pltpu.VMEM((128, 2048), BF16), in_...  78.7 us

profile of v5, /device:TPU:1, one launch (start us, length us, event | category | flops | bytes accessed | tf_op | source)
XLA Modules:
  0.0 79.5 jit_solution(14420286928810623939)
XLA Ops:
  0.0 78.7 %shard_map.145 = bf16[128,2048]{1,0:T(8,128)(2,1)S(1)} custom-call(bf16[128,2048]{1,0:T(8,128)(2,1)} %resid_hbm.1, bf16[512,512]{1,0:T(8,128)(2,1)} %query_hbm.1, bf16[512,512]{1,0:T(8,128)(2,1)} %forget_hbm.1, f32[1,512]{1,0:T(1,128)} %bitcast.8, f32[4,512]{1,0:T(4,128)} %bitcast.6, bf16[512,512]{1,0:T(8,128)(2,1)} %value_hbm.1, ...), custom_call_target="tpu_custom_call" | custom-call | tf_op jit(solution)/shard_map/pallas_call | solution.py:467
  78.7 0.8 %copy.17 = bf16[128,2048]{1,0:T(8,128)(2,1)} copy(bf16[128,2048]{1,0:T(8,128)(2,1)S(1)} %shard_map.145) | data formatting | bytes 1048576

commit v6 on v5

--- a/solution.py
+++ b/solution.py
@@ -292,7 +292,7 @@
 
         @pl.loop(low, top)
         def _(d):
-            p = wrap(me + d, 32)
+            p = (me + d * 11) % 32
             pltpu.make_async_remote_copy(
                 state_out.at[p], state_in.at[me], send, recv, sp_peer(p), MESH
             ).start()
@@ -328,7 +328,7 @@
 
         @pl.loop(low, top)
         def _(d):
-            p = wrap(me + d, 32)
+            p = (me + d * 11) % 32
             pltpu.make_async_remote_copy(
                 prior_out.at[p], prior_in.at[me], back[0], back[1], sp_peer(p), MESH
             ).start()

time: 79.6 us -> 79.3 us (level)
  no operation moved by 1% of the time
where the time goes in v6:
time: 79.3 us; the launch traced here: 79.2 us
  Pallas kernels  78.4 us (99%)
  local copies, waits for them, and re-layouts  0.8 us (1%)
    pallas_call x1, Pallas kernels, layer(): pl.pallas_call(layer_kernel, out_shape=pltpu.VMEM((128, 2048), BF16), in_...  78.4 us

profile of v6, /device:TPU:1, one launch (start us, length us, event | category | flops | bytes accessed | tf_op | source)
XLA Modules:
  0.0 79.2 jit_solution(13552059977801171917)
XLA Ops:
  0.0 78.4 %shard_map.145 = bf16[128,2048]{1,0:T(8,128)(2,1)S(1)} custom-call(bf16[128,2048]{1,0:T(8,128)(2,1)} %resid_hbm.1, bf16[512,512]{1,0:T(8,128)(2,1)} %query_hbm.1, bf16[512,512]{1,0:T(8,128)(2,1)} %forget_hbm.1, f32[1,512]{1,0:T(1,128)} %bitcast.8, f32[4,512]{1,0:T(4,128)} %bitcast.6, bf16[512,512]{1,0:T(8,128)(2,1)} %value_hbm.1, ...), custom_call_target="tpu_custom_call" | custom-call | tf_op jit(solution)/shard_map/pallas_call | solution.py:467
  78.4 0.8 %copy.17 = bf16[128,2048]{1,0:T(8,128)(2,1)} copy(bf16[128,2048]{1,0:T(8,128)(2,1)S(1)} %shard_map.145) | data formatting | bytes 1048576
